TPU v7x, 256 devices: a whole 4x4x8 slice. The times are simulated.
256 devices in a mesh: dp: 4 (over x), kv: 32 (over z, y), tp: 2 (over core).
Axes of the slice: x: 4, y: 4, z: 8, core: 2. Of those that a mesh axis runs over, the one named last changes fastest.
Arguments:
- tokens: bfloat16 [768, 4096], P('dp', ('kv', 'tp')), may hold values from -10 to 10
- gain_mixer: bfloat16 [4096], replicated, may hold values from 0.099609375 to 1.8984375
- weight_query: bfloat16 [4096, 16, 128], P('kv', 'tp'), may hold values from -0.09375 to 0.09375
- weight_key: bfloat16 [4096, 16, 128], P('kv', 'tp'), may hold values from -0.09375 to 0.09375
- weight_value: bfloat16 [4096, 16, 128], P('kv', 'tp'), may hold values from -0.09375 to 0.09375
- weight_outgate: bfloat16 [4096, 16, 128], P('kv', 'tp'), may hold values from -0.09375 to 0.09375
- weight_ingate: bfloat16 [4096, 16], replicated, may hold values from -0.09375 to 0.09375
- weight_forget: bfloat16 [4096, 16], replicated, may hold values from -0.09375 to 0.09375
- bias_input: float32 [16], replicated, may hold values from -3 to 3
- bias_forget: float32 [16], replicated, may hold values from 0 to 5
- memory: float32 [768, 16, 128, 128], P(('dp', 'kv'), 'tp'), may hold values from -2.5 to 2.5
- normalizer: float32 [768, 16, 128], P(('dp', 'kv'), 'tp'), may hold values from -2.5 to 2.5
- stabilizer: float32 [768, 16], P(('dp', 'kv'), 'tp'), may hold values from -1 to 3
- head_gain: bfloat16 [16, 128], replicated, may hold values from 0.099609375 to 1.8984375
- weight_out: bfloat16 [2048, 4096], P('tp', 'kv'), may hold values from -0.125 to 0.125
- gain_channel: bfloat16 [4096], replicated, may hold values from 0.099609375 to 1.8984375
- weight_up: bfloat16 [4096, 16384], P(None, ('kv', 'tp')), may hold values from -0.09375 to 0.09375
- weight_down: bfloat16 [16384, 4096], P(('kv', 'tp')), may hold values from -0.125 to 0.125
Outputs:
- layer_out: bfloat16 [768, 4096], P('dp', ('kv', 'tp'))
- new_memory: float32 [768, 16, 128, 128], P(('dp', 'kv'), 'tp')
- new_normalizer: float32 [768, 16, 128], P(('dp', 'kv'), 'tp')
- new_stabilizer: float32 [768, 16], P(('dp', 'kv'), 'tp')
All inputs are finite; a program needn't handle non-finite values.
Results may differ from a plain program's by a relative error of at most 0.017.
Values may be sent and summed in bfloat16 or wider, within the bound.
A program may use at most 64 MiB of HBM per device.

v0:
```python
import jax
import jax.numpy as jnp
from jax import lax
from jax.sharding import Mesh
from jax.sharding import PartitionSpec as P

KV = ("kv_0", "kv_1")
KV_TP = ("kv_0", "kv_1", "tp")
DP_KV = ("dp", "kv_0", "kv_1")


epsilon = 1e-06


def sent_to_all(value, axis):
    count = lax.axis_size(axis)
    return lax.all_to_all(
        jnp.broadcast_to(value[None], (count, *value.shape)), axis, 0, 0, tiled=True
    )


def laid_out(tiles, dim):
    tiles = jnp.moveaxis(tiles, 0, dim)
    dims = tiles.shape
    return tiles.reshape(*dims[:dim], dims[dim] * dims[dim + 1], *dims[dim + 2 :])


def gather_directly(value, axis, dim):
    tiles = sent_to_all(value, axis)
    return laid_out(tiles, dim)


def in_one_piece(arrays, axis, split_dim, concat_dim, along):
    widths = [a.shape[along] for a in arrays]
    both = jnp.concatenate(arrays, axis=along)
    result = lax.all_to_all(both, axis, split_axis=split_dim, concat_axis=concat_dim, tiled=True)
    return tuple(jnp.split(result, [sum(widths[:k]) for k in range(1, len(widths))], axis=along))


def whole_of(value, axes, dim):
    if not axes:
        return value
    nearer = lax.all_gather(value, axes[-1], axis=dim, tiled=True)
    return whole_of(nearer, axes[:-1], dim)


def split_up(value, dim, count):
    dims = value.shape
    tiles = value.reshape(*dims[:dim], count, dims[dim] // count, *dims[dim + 1 :])
    return jnp.moveaxis(tiles, dim, 0)


def sent_and_summed(value, axis, dim):
    tiles = split_up(value, dim, lax.axis_size(axis))
    arrived = lax.all_to_all(tiles, axis, split_axis=0, concat_axis=0, tiled=True)
    return arrived.astype(jnp.float32).sum(axis=0)


def all_blocks(value, axes, sequence):
    tiles = value
    for k in sequence:
        tiles = lax.all_gather(tiles, axes[k])
    done = sequence[::-1]
    back = [done.index(k) for k in range(len(axes))]
    tiles = tiles.transpose(*back, *range(len(axes), tiles.ndim))
    return tiles.reshape(-1, *value.shape)


def gather_axes(value, axes, sequence, dim):
    return laid_out(all_blocks(value, axes, sequence), dim)


def project(scaled, weight):
    return jnp.dot(scaled, weight.reshape(weight.shape[0], -1), preferred_element_type=jnp.float32)


def scale_slab(slab_rows, gain):
    rows_wide = slab_rows.astype(jnp.float32)
    gain_slice = gain.astype(jnp.float32)
    return ((rows_wide * gain_slice).astype(jnp.bfloat16), jnp.sum(rows_wide * rows_wide, axis=1))


def cell_update(
    queries,
    keys_in,
    values_in,
    outgates,
    ingate,
    forget,
    memory,
    normalizer,
    stabilizer,
    head_scale,
):
    head_dim = queries.shape[-1]
    query_wide = queries.astype(jnp.float32)
    key_scaled = keys_in.astype(jnp.float32) * head_dim ** (-0.5)
    value_wide = values_in.astype(jnp.float32)
    new_stabilizer = jnp.maximum(forget + stabilizer, ingate)
    retain = jnp.exp(forget + stabilizer - new_stabilizer)
    inflow = jnp.exp(ingate - new_stabilizer)
    new_memory = (
        retain[..., None, None] * memory
        + (inflow[..., None] * value_wide)[..., :, None] * key_scaled[..., None, :]
    )
    new_normalizer = retain[..., None] * normalizer + inflow[..., None] * key_scaled
    numerator = jnp.einsum("bhvk,bhk->bhv", new_memory, query_wide, precision=lax.Precision.HIGHEST)
    denominator = jnp.sum(new_normalizer * query_wide, axis=-1)
    readout = numerator / jnp.maximum(jnp.abs(denominator), jnp.exp(-new_stabilizer))[..., None]
    centered = readout - jnp.mean(readout, axis=-1, keepdims=True)
    normed = centered * lax.rsqrt(jnp.mean(centered * centered, axis=-1, keepdims=True) + epsilon)
    gated_out = (
        normed * head_scale.astype(jnp.float32) * jax.nn.sigmoid(outgates.astype(jnp.float32))
    )
    return (gated_out.astype(jnp.bfloat16), new_memory, new_normalizer, new_stabilizer)


def body(
    tokens,
    gain_mixer,
    weight_query,
    weight_key,
    weight_value,
    weight_outgate,
    weight_ingate,
    weight_forget,
    bias_input,
    bias_forget,
    memory,
    normalizer,
    stabilizer,
    head_gain,
    weight_out,
    gain_channel,
    weight_up,
    weight_down,
):
    kv_rank = lax.axis_index(KV)
    tp_rank = lax.axis_index("tp")
    own_rows = memory.shape[0]
    heads_here = memory.shape[1]
    head_dim = memory.shape[2]
    width_full = gain_mixer.shape[0]
    rows_total = tokens.shape[0]
    head_start = tp_rank * heads_here
    gate_weights = jnp.concatenate(
        [
            lax.dynamic_slice_in_dim(weight_ingate, head_start, heads_here, 1),
            lax.dynamic_slice_in_dim(weight_forget, head_start, heads_here, 1),
        ],
        axis=1,
    )
    slab_rows = gather_directly(tokens, "tp", 1)
    local_weights = in_one_piece(
        (weight_query, weight_key, weight_value, weight_outgate), KV, 2, 0, 1
    )
    scaled, squares = scale_slab(whole_of(slab_rows, KV, 1), gain_mixer)
    sums = tuple((project(scaled, weight) for weight in local_weights))
    gate_sum = jnp.dot(scaled, gate_weights, preferred_element_type=jnp.float32)
    folded = sums + (gate_sum, squares)
    inverse_all = lax.rsqrt(folded[5] / width_full + epsilon)[:, None]
    thin_parts = tuple(
        (
            (inverse_all * folded[member]).astype(jnp.bfloat16).reshape(rows_total, heads_here, -1)
            for member in range(4)
        )
    )
    queries, keys_proj, values_proj, outgates = in_one_piece(
        (thin_parts[0], thin_parts[1], thin_parts[2], thin_parts[3]), KV, 0, 2, 1
    )
    gate_pre = lax.dynamic_slice_in_dim(inverse_all * folded[4], kv_rank * own_rows, own_rows, 0)
    ingate = gate_pre[:, :heads_here] + lax.dynamic_slice_in_dim(
        bias_input, head_start, heads_here, 0
    )
    forget = jax.nn.log_sigmoid(
        gate_pre[:, heads_here:] + lax.dynamic_slice_in_dim(bias_forget, head_start, heads_here, 0)
    )
    head_scale = lax.dynamic_slice_in_dim(head_gain, head_start, heads_here, 0)
    heads_out, new_memory, new_normalizer, new_stabilizer = cell_update(
        queries,
        keys_proj,
        values_proj,
        outgates,
        ingate,
        forget,
        memory,
        normalizer,
        stabilizer,
        head_scale,
    )
    heads_flat = heads_out.reshape(own_rows, heads_here * head_dim)
    partial_out = jnp.dot(
        gather_directly(heads_flat, KV, 0), weight_out, preferred_element_type=jnp.float32
    ).astype(jnp.bfloat16)
    partial_wide = lax.optimization_barrier(partial_out).astype(jnp.float32)
    projected = sent_and_summed(partial_wide.astype(jnp.bfloat16), "tp", 1)
    mixed_rows = (tokens.astype(jnp.float32) + projected).astype(jnp.bfloat16)
    scaled_mlp, squares_mlp = scale_slab(gather_axes(mixed_rows, KV_TP, (1, 0, 2), 1), gain_channel)
    weight_block = weight_up
    up_total = jnp.dot(scaled_mlp, weight_block, preferred_element_type=jnp.float32)
    inverse_mlp = lax.rsqrt(squares_mlp / width_full + epsilon)[:, None]
    activation = jax.nn.relu(inverse_mlp * up_total)
    squared = (activation * activation).astype(jnp.bfloat16)
    weight_block = weight_down
    transposed = sent_and_summed(
        jnp.einsum("uc,ru->cr", weight_block, squared, preferred_element_type=jnp.float32).astype(
            jnp.bfloat16
        ),
        KV_TP,
        0,
    )
    layer_out = (mixed_rows.astype(jnp.float32) + transposed.T).astype(jnp.bfloat16)
    return (layer_out, new_memory, new_normalizer, new_stabilizer)


def solution(mesh):
    torus = Mesh(
        mesh.devices.reshape(mesh.shape["dp"], 8, 4, mesh.shape["tp"]), ("dp", "kv_0", "kv_1", "tp")
    )
    placed = (
        P("dp", KV_TP),
        P(),
        P(KV, "tp", None),
        P(KV, "tp", None),
        P(KV, "tp", None),
        P(KV, "tp", None),
        P(),
        P(),
        P(),
        P(),
        P(DP_KV, "tp", None, None),
        P(DP_KV, "tp", None),
        P(DP_KV, "tp"),
        P(),
        P("tp", KV),
        P(),
        P(None, KV_TP),
        P(KV_TP, None),
    )
    return jax.shard_map(
        body,
        mesh=torus,
        in_specs=placed,
        out_specs=(
            P("dp", KV_TP),
            P(DP_KV, "tp", None, None),
            P(DP_KV, "tp", None),
            P(DP_KV, "tp"),
        ),
        check_vma=False,
    )
```

profile of v0, /device:TPU:1, one launch (start us, length us, event | category | flops | bytes accessed | tf_op | source)
XLA Modules:
  0.0 289.6 jit_solution(11860012155825132862)
XLA Ops:
  8.7 6.5 %all-to-all-start = ((bf16[2,192,64]{1,2,0:T(8,128)(2,1)}), bf16[2,192,64]{1,2,0:T(8,128)(2,1)S(1)}, u32[]{:S(2)}, u32[]{:S(2)}) async-start(bf16[2,192,64]{1,2,0:T(8,128)(2,1)} %broadcast_in_dim.6), calls=%async_computation | async-start | bytes 131072 | tf_op jit(solution)/shard_map/all_to_all | solution.py:17
  21.3 9.5 %all-to-all-start.1 = ((bf16[128,32,128]{0,1,2:T(8,128)(2,1)}), bf16[128,32,128]{0,1,2:T(8,128)(2,1)S(1)}, u32[]{:S(2)}, u32[]{:S(2)}) async-start(bf16[128,32,128]{0,1,2:T(8,128)(2,1)} %pad_maximum_fusion), calls=%async_computation.1 | async-start | bytes 2097152 | tf_op jit(solution)/shard_map/all_to_all | solution.py:36
  30.8 14.1 %all_gather.24 = bf16[192,512]{0,1:T(8,128)(2,1)} all-gather(bf16[192,128]{0,1:T(8,128)(2,1)S(1)} %bitcast.95), channel_id=1, replica_groups=mesh['dp'=4,'kv_0'=8,'kv_1'=4,'tp'=2] {'kv_1'}, dimensions={1}, use_global_device_ids=true | all-gather | bytes 245760 | tf_op jit(solution)/shard_map/all_gather | solution.py:43
  47.6 10.4 %all-to-all-done.1 = bf16[128,32,128]{0,1,2:T(8,128)(2,1)S(1)} async-done(((bf16[128,32,128]{0,1,2:T(8,128)(2,1)}), bf16[128,32,128]{0,1,2:T(8,128)(2,1)S(1)}, u32[]{:S(2)}, u32[]{:S(2)}) %all-to-all-start.1) | async-done | bytes 1048608 | tf_op jit(solution)/shard_map/all_to_all | solution.py:36
  61.2 23.1 %all-gather.7.cloned.1.call-done = bf16[192,4096]{0,1:T(8,128)(2,1)} async-done(((bf16[192,512]{0,1:T(8,128)(2,1)}), bf16[192,4096]{0,1:T(8,128)(2,1)}) %all-gather.7.cloned.1.call-update) | async-done | bytes 1572880 | tf_op jit(solution)/shard_map/all_gather | solution.py:43
  84.3 2.0 fusion.1
  88.3 2.1 fusion.11
  90.5 2.1 fusion.10
  92.8 2.1 fusion.9
  96.5 6.6 %all-to-all-start.2 = ((bf16[32,2,384]{2,1,0:T(2,128)(2,1)}), bf16[32,2,384]{2,1,0:T(2,128)(2,1)S(1)}, u32[]{:S(2)}, u32[]{:S(2)}) async-start(bf16[32,2,384]{2,1,0:T(2,128)(2,1)} %reshape.111), calls=%async_computation.2 | async-start | bytes 98304 | tf_op jit(solution)/shard_map/all_to_all | solution.py:36
  103.4 8.4 %all-to-all-done.2 = bf16[32,2,384]{2,1,0:T(2,128)(2,1)S(1)} async-done(((bf16[32,2,384]{2,1,0:T(2,128)(2,1)}), bf16[32,2,384]{2,1,0:T(2,128)(2,1)S(1)}, u32[]{:S(2)}, u32[]{:S(2)}) %all-to-all-start.2) | async-done | bytes 49184 | tf_op jit(solution)/shard_map/all_to_all | solution.py:36
  116.6 2.5 multiply_add_fusion
  120.7 2.5 fusion.32
  123.8 15.9 %all_to_all.56 = bf16[32,6,1024]{2,1,0:T(8,128)(2,1)S(1)} all-to-all(bf16[32,6,1024]{2,1,0:T(8,128)(2,1)S(1)} %broadcast_in_dim.8), channel_id=1, replica_groups=mesh['dp'=4,'kv_0'=8,'kv_1'=4,'tp'=2] {'kv_0','kv_1'}, dimensions={0} | all-to-all | bytes 786432 | tf_op jit(solution)/shard_map/all_to_all | solution.py:17
  141.2 10.9 %all_to_all.57 = bf16[2,192,64]{1,2,0:T(8,128)(2,1)S(1)} all-to-all(bf16[2,192,64]{1,2,0:T(8,128)(2,1)S(1)} %bitcast.96), channel_id=1, replica_groups=mesh['dp'=4,'kv_0'=8,'kv_1'=4,'tp'=2] {'tp'}, dimensions={0} | all-to-all | bytes 98304 | tf_op jit(solution)/shard_map/all_to_all | solution.py:55
  152.1 9.1 %all-gather.3 = bf16[4,192,64]{1,2,0:T(8,128)(2,1)S(1)} all-gather(bf16[1,192,64]{1,2,0:T(8,128)(2,1)S(1)} %fusion.26), channel_id=2, replica_groups=mesh['dp'=4,'kv_0'=8,'kv_1'=4,'tp'=2] {'kv_1'}, dimensions={0}, use_global_device_ids=true | all-gather | bytes 122880 | tf_op jit(solution)/shard_map/all_gather | solution.py:62
  161.3 23.5 %all-gather.1 = bf16[32,192,64]{1,2,0:T(8,128)(2,1)} all-gather(bf16[4,192,64]{1,2,0:T(8,128)(2,1)S(1)} %all-gather.3), channel_id=3, replica_groups=mesh['dp'=4,'kv_0'=8,'kv_1'=4,'tp'=2] {'kv_0'}, dimensions={0}, use_global_device_ids=true | all-gather | bytes 884736 | tf_op jit(solution)/shard_map/all_gather | solution.py:62
  184.8 21.0 %all-gather.9.cloned.1.call-done = bf16[16,4,192,64]{2,3,1,0:T(8,128)(2,1)} async-done(((bf16[8,4,192,64]{2,3,1,0:T(8,128)(2,1)}), bf16[16,4,192,64]{2,3,1,0:T(8,128)(2,1)}) %all-gather.9.cloned.1.call-update) | async-done | bytes 1572880 | tf_op jit(solution)/shard_map/all_gather | solution.py:62
  205.9 2.3 fusion.3
  209.3 2.0 fusion.4
  211.2 5.2 %fusion = bf16[4096,192]{0,1:T(8,128)(2,1)} fusion(bf16[256,4096]{1,0:T(8,128)(2,1)S(1)} %copy-done, bf16[192,4096]{0,1:T(8,128)(2,1)} %fusion.4, bf16[4096,256]{1,0:T(8,128)(2,1)} %param.34, f32[192]{0:T(256)S(1)} %add_rsqrt_fusion.1), kind=kOutput, calls=%fused_computation.5 | convolution fusion | flops 806289408 | bytes 7340800 | tf_op jit(solution)/shard_map/uc,ru->cr/dot_general | solution.py:206
  216.5 3.9 %copy.165 = bf16[4096,192]{1,0:T(8,128)(2,1)} copy(bf16[4096,192]{0,1:T(8,128)(2,1)} %fusion) | data formatting | bytes 3145728 | tf_op jit(solution)/shard_map/convert_element_type | solution.py:206
  220.4 10.2 %all-to-all-start.5 = ((bf16[64,64,192]{2,1,0:T(8,128)(2,1)}), bf16[64,64,192]{2,1,0:T(8,128)(2,1)}, u32[]{:S(2)}, u32[]{:S(2)}) async-start(bf16[64,64,192]{2,1,0:T(8,128)(2,1)} %bitcast.85), calls=%async_computation.5 | async-start | bytes 4194304 | tf_op jit(solution)/shard_map/all_to_all | solution.py:55
  231.3 48.9 %all-to-all-done.5 = bf16[64,64,192]{2,1,0:T(8,128)(2,1)} async-done(((bf16[64,64,192]{2,1,0:T(8,128)(2,1)}), bf16[64,64,192]{2,1,0:T(8,128)(2,1)}, u32[]{:S(2)}, u32[]{:S(2)}) %all-to-all-start.5) | async-done | bytes 1572896 | tf_op jit(solution)/shard_map/all_to_all | solution.py:55
  (108 shorter events, 30.2 us)
Async XLA Ops:
  7.2 204.1 %copy-start = (bf16[256,4096]{1,0:T(8,128)(2,1)S(1)}, bf16[256,4096]{1,0:T(8,128)(2,1)}, u32[]{:S(2)}) copy-start(bf16[256,4096]{1,0:T(8,128)(2,1)} %param.35) | copy-start | bytes 6291460
  8.7 12.6 %all-to-all-start = ((bf16[2,192,64]{1,2,0:T(8,128)(2,1)}), bf16[2,192,64]{1,2,0:T(8,128)(2,1)S(1)}, u32[]{:S(2)}, u32[]{:S(2)}) async-start(bf16[2,192,64]{1,2,0:T(8,128)(2,1)} %broadcast_in_dim.6), calls=%async_computation | async-start | bytes 131072 | tf_op jit(solution)/shard_map/all_to_all | solution.py:17
  20.0 24.9 %copy-start.15 = (f32[16]{0:T(128)S(1)}, f32[16]{0:T(128)}, u32[]{:S(2)}) copy-start(f32[16]{0:T(128)} %param.27) | copy-start | bytes 196
  20.1 25.5 %copy-start.16 = (f32[16]{0:T(128)S(1)}, f32[16]{0:T(128)}, u32[]{:S(2)}) copy-start(f32[16]{0:T(128)} %param.26) | copy-start | bytes 196
  20.1 26.1 %copy-start.10 = (bf16[4096]{0:T(1024)(128)(2,1)S(1)}, bf16[4096]{0:T(1024)(128)(2,1)}, u32[]{:S(2)}) copy-start(bf16[4096]{0:T(1024)(128)(2,1)} %param.19) | copy-start | bytes 24580
  20.1 26.1 %copy-start.13 = (bf16[16,128]{1,0:T(8,128)(2,1)S(1)}, bf16[16,128]{1,0:T(8,128)(2,1)}, u32[]{:S(2)}) copy-start(bf16[16,128]{1,0:T(8,128)(2,1)} %param.31) | copy-start | bytes 12292
  20.1 26.7 %copy-start.6 = (bf16[4096,16]{0,1:T(8,128)(2,1)S(1)}, bf16[4096,16]{0,1:T(8,128)(2,1)}, u32[]{:S(2)}) copy-start(bf16[4096,16]{0,1:T(8,128)(2,1)} %param.25) | copy-start | bytes 393220
  21.3 36.8 %all-to-all-start.1 = ((bf16[128,32,128]{0,1,2:T(8,128)(2,1)}), bf16[128,32,128]{0,1,2:T(8,128)(2,1)S(1)}, u32[]{:S(2)}, u32[]{:S(2)}) async-start(bf16[128,32,128]{0,1,2:T(8,128)(2,1)} %pad_maximum_fusion), calls=%async_computation.1 | async-start | bytes 2097152 | tf_op jit(solution)/shard_map/all_to_all | solution.py:36
  30.8 53.5 %all-gather.7.cloned.1.call-start = ((), (), s32[]{:S(2)}) async-start(), calls=%async_computation.6 | async-start | bytes 2359296 | tf_op jit(solution)/shard_map/all_gather | solution.py:43
  86.3 1.3 copy-start.1
  86.3 1.0 copy-start.9
  86.3 0.9 copy-start.12
  86.3 0.9 copy-start.14
  87.3 25.9 %copy-start.5 = (f32[6,8]{1,0:T(8,128)}, f32[6,8]{1,0:T(8,128)S(1)}, u32[]{:S(2)}) copy-start(f32[6,8]{1,0:T(8,128)S(1)} %get-tuple-element.32) | copy-start | bytes 580
  92.6 10.5 %copy-start.7 = (f32[6,8,128]{2,1,0:T(8,128)S(1)}, f32[6,8,128]{2,1,0:T(8,128)}, u32[]{:S(2)}) copy-start(f32[6,8,128]{2,1,0:T(8,128)} %param.29) | copy-start | bytes 73732
  96.5 15.3 %all-to-all-start.2 = ((bf16[32,2,384]{2,1,0:T(2,128)(2,1)}), bf16[32,2,384]{2,1,0:T(2,128)(2,1)S(1)}, u32[]{:S(2)}, u32[]{:S(2)}) async-start(bf16[32,2,384]{2,1,0:T(2,128)(2,1)} %reshape.111), calls=%async_computation.2 | async-start | bytes 98304 | tf_op jit(solution)/shard_map/all_to_all | solution.py:36
  103.1 102.8 %all-gather.9.cloned.1.call-start = ((), (), s32[]{:S(2)}) async-start(), calls=%async_computation.7 | async-start | bytes 3145728 | tf_op jit(solution)/shard_map/all_gather | solution.py:62
  119.1 1.7 copy-start.2
  120.7 2.9 %copy-start.8 = (f32[8,128]{1,0:T(8,128)S(1)}, f32[8,128]{1,0:T(8,128)}, u32[]{:S(2)}) copy-start(f32[8,128]{1,0:T(8,128)} %dynamic-slice_convert_fusion) | copy-start | bytes 12292
  123.3 28.9 %copy-start.4 = (bf16[192,64]{0,1:T(8,128)(2,1)S(1)}, bf16[192,64]{0,1:T(8,128)(2,1)}, u32[]{:S(2)}) copy-start(bf16[192,64]{0,1:T(8,128)(2,1)} %param.18) | copy-start | bytes 73732
  139.7 45.1 %copy-start.11 = (bf16[4096]{0:T(1024)(128)(2,1)S(1)}, bf16[4096]{0:T(1024)(128)(2,1)}, u32[]{:S(2)}) copy-start(bf16[4096]{0:T(1024)(128)(2,1)} %param.33) | copy-start | bytes 24580
  205.9 2.3 copy-start.3
  220.4 59.8 %all-to-all-start.5 = ((bf16[64,64,192]{2,1,0:T(8,128)(2,1)}), bf16[64,64,192]{2,1,0:T(8,128)(2,1)}, u32[]{:S(2)}, u32[]{:S(2)}) async-start(bf16[64,64,192]{2,1,0:T(8,128)(2,1)} %bitcast.85), calls=%async_computation.5 | async-start | bytes 4194304 | tf_op jit(solution)/shard_map/all_to_all | solution.py:55
Sparse Core Ops, SparseCore 0:
  45.1 39.1 all-gather.6
  184.9 20.8 all-gather.8
where the time goes:
time: 291 us; the launch traced here: 290 us
  waiting for transfers between devices  112 us (38%)
  blocking collectives  73.6 us (25%)
  starting transfers between devices  32.8 us (11%)
  local copies, waits for them, and re-layouts  25 us (9%)
  matrix products  16.4 us (6%)
  other arithmetic  15.4 us (5%)
  between operations  14.6 us (5%)
    all_to_all x1, waiting for transfers between devices, sent_and_summed(): lax.all_to_all(tiles, axis, split_axis=0, concat_axis=0, tiled=True)  48.9 us
    all_gather x2, blocking collectives, all_blocks(): tiles = lax.all_gather(tiles, axes[k])  32.6 us
    all_gather x1, waiting for transfers between devices, whole_of(): nearer = lax.all_gather(value, axes[-1], axis=dim, tiled=True)  23.1 us
    all_gather x1, waiting for transfers between devices, all_blocks(): tiles = lax.all_gather(tiles, axes[k])  21 us
    all_to_all x2, waiting for transfers between devices, in_one_piece(): lax.all_to_all(both, axis, split_axis=split_dim, concat_axis=concat_dim,...  18.9 us
    all_to_all x2, starting transfers between devices, in_one_piece(): lax.all_to_all(both, axis, split_axis=split_dim, concat_axis=concat_dim,...  16.1 us
    all_to_all x1, blocking collectives, sent_to_all(): lax.all_to_all(jnp.broadcast_to(value[None], (count, *value.shape)), axis...  15.9 us
    all_gather x1, blocking collectives, whole_of(): nearer = lax.all_gather(value, axes[-1], axis=dim, tiled=True)  14.1 us
  transfers between devices with their start and end apart: 6, of which 5 were waited for; matrix products, arithmetic and copies ran while one was open for 4% of the time, Pallas kernels for 0%

commit v1 on v0

v1 whole, which is shorter than its diff:
```python
import functools

import jax
import jax.numpy as jnp
from jax import lax
from jax.experimental import pallas as pl
from jax.experimental.pallas import tpu as pltpu
from jax.sharding import Mesh
from jax.sharding import PartitionSpec as P

EPS = 1e-06
KV_TP = ("z", "y", "tp")
KV = ("z", "y")
DP_KV = ("dp", "z", "y")
MESH = pl.DeviceIdType.MESH
F32 = jnp.float32
BF16 = jnp.bfloat16


def by_distance(n):
    return sorted(range(1, n), key=lambda d: (min(d, n - d), d))


def kernel(
    nz,
    ny,
    width_full,
    tokens,
    gain_mixer,
    w0,
    w1,
    w2,
    w3,
    w_in,
    w_forget,
    bias_in,
    bias_forget,
    memory,
    normalizer,
    stabilizer,
    head_gain,
    w_out,
    gain_channel,
    w_up,
    w_down,
    out,
    inflow_v_out,
    key_out,
    retain_out,
    norm_out,
    stab_out,
    tok_in,
    tok_half,
    tok_all,
    gains,
    wig,
    wfg,
    mem,
    wbuf,
    wide,
    w_flat,
    partial,
    part_send,
    part_recv,
    gate_send,
    gate_recv,
    rows_send,
    rows_recv,
    q_f32,
    mq,
    heads_own,
    heads_all,
    heads_f32,
    wo_all,
    up_all,
    down_all,
    mixed_all,
    acc,
    down_send,
    down_y,
    sum_send,
    sum_recv,
    fin_send,
    fin_recv,
    local_sem,
    pair_send,
    pair_recv,
    wy_send,
    wy_recv,
    ty_send,
    ty_recv,
    pz_send,
    pz_recv,
    gz_send,
    gz_recv,
    ry_send,
    ry_recv,
    hz_send,
    hz_recv,
    hy_send,
    hy_recv,
    mz_send,
    mz_recv,
    my_send,
    my_recv,
    dy_send,
    dy_recv,
    dz_send,
    dz_recv,
):
    z = lax.axis_index("z")
    y = lax.axis_index("y")
    tp = lax.axis_index("tp")
    other = 1 - tp
    half_z = nz // 2
    rows = tokens.shape[0]
    half = rows // 2
    own = 6
    heads = 8
    zrows = ny * own
    block = ny * 128
    near_z = by_distance(nz)
    near_y = by_distance(ny)
    far_z = near_z[::-1]
    pending = []

    def remote(src, dst, send, recv, **to):
        return pltpu.make_async_remote_copy(
            src_ref=src, dst_ref=dst, send_sem=send, recv_sem=recv, device_id=to, device_id_type=MESH
        )

    def push(*args, **to):
        copy = remote(*args, **to)
        copy.start()
        pending.append(copy)
        return copy

    barrier = pltpu.get_barrier_semaphore()
    for d in near_z:
        for t in range(2):
            pl.semaphore_signal(
                barrier, inc=1, device_id={"z": (z + d) % nz, "tp": t}, device_id_type=MESH
            )
    for d in near_y:
        pl.semaphore_signal(barrier, inc=1, device_id={"y": (y + d) % ny}, device_id_type=MESH)
    pl.semaphore_signal(barrier, inc=1, device_id={"tp": other}, device_id_type=MESH)

    rows_of_block = pl.ds(pl.multiple_of(z * block, block), block)
    loads = [
        pltpu.make_async_copy(w_in.at[rows_of_block], wig, local_sem.at[0]),
        pltpu.make_async_copy(w_forget.at[rows_of_block], wfg, local_sem.at[1]),
        pltpu.make_async_copy(memory, mem, local_sem.at[2]),
        pltpu.make_async_copy(w_out, wo_all.at[tp], local_sem.at[3]),
        pltpu.make_async_copy(w_up, up_all.at[tp], local_sem.at[4]),
        pltpu.make_async_copy(w_down, down_all.at[tp], local_sem.at[5]),
    ]
    weights = (w0, w1, w2, w3)
    for m in range(4):

        @pl.when(y == m)
        def _(m=m):
            pltpu.make_async_copy(weights[m], wbuf.at[m], local_sem.at[6]).start()

    for copy in loads:
        copy.start()
    gains[0] = gain_mixer[...].astype(F32)
    gains[1] = gain_channel[...].astype(F32)

    pl.semaphore_wait(barrier, 2 * (nz - 1) + (ny - 1) + 1)

    tok_copy = push(tokens, tok_in, pair_send.at[0], pair_recv.at[0], tp=other)
    for m in range(4):

        @pl.when(y != m)
        def _(m=m):
            remote(weights[m], wbuf.at[y], wy_send.at[m], wy_recv.at[y], y=m).start()

    out_copy = push(w_out, wo_all.at[tp], pair_send.at[1], pair_recv.at[1], tp=other)
    up_copy = push(w_up, up_all.at[tp], pair_send.at[2], pair_recv.at[2], tp=other)
    down_copy = push(w_down, down_all.at[tp], pair_send.at[3], pair_recv.at[3], tp=other)

    tok_copy.wait_recv()
    mine, theirs = tokens[...].astype(F32), tok_in[...].astype(F32)
    first = jnp.where(tp == 0, mine, theirs)
    second = jnp.where(tp == 0, theirs, mine)
    chip = jnp.concatenate([first, second], axis=1).astype(BF16)
    tok_all[y] = chip
    tok_half[0] = chip[:half]
    tok_half[1] = chip[half:]
    for d in near_y:
        push(
            tok_all.at[y], tok_all.at[y], ty_send.at[d], ty_recv.at[y], y=(y + d) % ny
        )
    for d in near_y:
        s = (y + d) % ny
        remote(tok_all.at[s], tok_all.at[s], ty_send.at[d], ty_recv.at[s], y=s).wait_recv()
    squares = jnp.zeros((rows, 1), F32)
    scaled = []
    for s in range(ny):
        wide_rows = tok_all[s].astype(F32)
        squares = squares + jnp.sum(wide_rows * wide_rows, axis=1, keepdims=True)
        scaled.append((wide_rows * gains[0, pl.ds(z * ny + s, 1), :]).astype(BF16))
    x = jnp.concatenate(scaled, axis=1)
    loads[0].wait()
    loads[1].wait()
    gate = jnp.concatenate(
        [
            jnp.dot(x, wig[...], preferred_element_type=F32),
            jnp.dot(x, wfg[...], preferred_element_type=F32),
            jnp.broadcast_to(squares, (rows, 96)),
        ],
        axis=1,
    )
    for k in range(nz):
        gate_send[k] = gate[k * zrows : (k + 1) * zrows]
    for d in far_z:
        to = (z + d) % nz
        push(gate_send.at[to], gate_recv.at[z], gz_send.at[d], gz_recv.at[z], z=to)

    def flatten(s):
        wide[...] = wbuf[s].astype(F32).reshape(128 * heads, 128)
        base = pl.multiple_of(s * 128, 128)
        for h in range(heads):
            w_flat[pl.ds(base, 128), h * 128 : (h + 1) * 128] = wide[
                pl.ds(h, 128, stride=heads), :
            ].astype(BF16)

    pltpu.make_async_copy(weights[0], wbuf.at[y], local_sem.at[6]).wait()
    flatten(y)
    for d in near_y:
        s = (y + d) % ny
        remote(wbuf.at[s], wbuf.at[s], wy_send.at[0], wy_recv.at[s], y=s).wait_recv()
        flatten(s)
    wcols = heads * 64
    for n in range(2):
        partial[n] = jnp.dot(
            x, w_flat[:, n * wcols : (n + 1) * wcols], preferred_element_type=F32
        )
    for k in range(nz):
        part_send[k] = jnp.concatenate(
            [
                partial[0, k * zrows : (k + 1) * zrows, :],
                partial[1, k * zrows : (k + 1) * zrows, :],
            ],
            axis=0,
        ).astype(BF16)
    for d in far_z:
        to = (z + d) % nz
        push(part_send.at[to], part_recv.at[z], pz_send.at[d], pz_recv.at[z], z=to)

    gate_sum = gate_send[z]
    for d in near_z:
        s = (z + d) % nz
        remote(gate_recv.at[s], gate_recv.at[s], gz_send.at[d], gz_recv.at[s], z=s).wait_recv()
        gate_sum = gate_sum + gate_recv[s]
    inverse = lax.rsqrt(gate_sum[:, 32:33] / width_full + EPS)
    gate_pre = inverse * gate_sum
    gate_rows = jnp.zeros((own, 128), F32)
    for k in range(ny):
        gate_rows = gate_rows + jnp.where(y == k, gate_pre[k * own : (k + 1) * own], 0.0)
    in_all = gate_rows[:, 0:16] + bias_in[...]
    forget_all = gate_rows[:, 16:32] + bias_forget[...]
    ingate = jnp.where(tp == 0, in_all[:, :8], in_all[:, 8:])
    forget_pre = jnp.where(tp == 0, forget_all[:, :8], forget_all[:, 8:])
    forget = jnp.minimum(forget_pre, 0.0) - jnp.log(1.0 + jnp.exp(-jnp.abs(forget_pre)))
    carried = forget + stabilizer[...]
    new_stab = jnp.maximum(carried, ingate)
    stab_out[...] = new_stab
    diagonal = lax.broadcasted_iota(jnp.int32, (heads, heads), 0) == lax.broadcasted_iota(
        jnp.int32, (heads, heads), 1
    )

    def column(value):
        return jnp.concatenate(
            [
                jnp.sum(
                    jnp.where(diagonal, jnp.broadcast_to(value[b : b + 1], (heads, heads)), 0.0),
                    axis=1,
                    keepdims=True,
                )
                for b in range(own)
            ],
            axis=0,
        )

    retain = column(jnp.exp(carried - new_stab))
    inflow = column(jnp.exp(ingate - new_stab))
    floor = column(jnp.exp(-new_stab))

    total = part_send[z].astype(F32)
    for d in near_z:
        s = (z + d) % nz
        remote(part_recv.at[s], part_recv.at[s], pz_send.at[d], pz_recv.at[s], z=s).wait_recv()
        total = total + part_recv[s].astype(F32)
    for h in range(heads):
        n, c = h // 4, h % 4
        rows_send[pl.ds(h, zrows, stride=heads), :] = inverse * total[
            n * zrows : (n + 1) * zrows, c * 128 : (c + 1) * 128
        ]
    piece = own * heads
    for d in near_y:
        to = (y + d) % ny
        push(
            rows_send.at[pl.ds(pl.multiple_of(to * piece, piece), piece)],
            rows_recv.at[y],
            ry_send.at[d],
            ry_recv.at[y],
            y=to,
        )
    rows_recv[y] = rows_send[pl.ds(pl.multiple_of(y * piece, piece), piece), :]
    for d in near_y:
        s = (y + d) % ny
        remote(rows_recv.at[s], rows_recv.at[s], ry_send.at[d], ry_recv.at[s], y=s).wait_recv()

    query = rows_recv[0].astype(BF16).astype(F32)
    key = rows_recv[1].astype(BF16).astype(F32) * 128**-0.5
    value = rows_recv[2].astype(BF16).astype(F32)
    gate_o = rows_recv[3].astype(BF16).astype(F32)
    q_f32[...] = query
    new_norm = retain * normalizer[...] + inflow * key
    norm_out[...] = new_norm
    inflow_value = inflow * value
    inflow_v_out[...] = inflow_value
    key_out[...] = key
    retain_out[...] = jnp.broadcast_to(retain, (piece, 128))
    loads[2].wait()
    sub = lax.broadcasted_iota(jnp.int32, (heads, 128), 0)
    contract = (((1,), (1,)), ((), ()))

    def readout_of(b, carry):
        q_b = q_f32[pl.ds(pl.multiple_of(b * heads, heads), heads), :].astype(BF16)
        found = jnp.zeros((heads, 128), F32)
        for h in range(heads):
            m_bh = mem[b * heads + h]
            high = m_bh.astype(BF16)
            low = (m_bh - high.astype(F32)).astype(BF16)
            product = lax.dot_general(
                q_b, high, contract, preferred_element_type=F32
            ) + lax.dot_general(q_b, low, contract, preferred_element_type=F32)
            found = jnp.where(sub == h, product, found)
        mq[pl.ds(pl.multiple_of(b * heads, heads), heads), :] = found
        return carry

    lax.fori_loop(0, own, readout_of, 0)
    numerator = retain * mq[...] + inflow_value * jnp.sum(key * query, axis=1, keepdims=True)
    denominator = jnp.sum(new_norm * query, axis=1, keepdims=True)
    readout = numerator / jnp.maximum(jnp.abs(denominator), floor)
    centered = readout - jnp.mean(readout, axis=1, keepdims=True)
    normed = centered * lax.rsqrt(jnp.mean(centered * centered, axis=1, keepdims=True) + EPS)
    gain_all = head_gain[...].astype(F32)
    gain_own = jnp.where(tp == 0, gain_all[:heads], gain_all[heads:])
    heads_out = (
        normed * jnp.concatenate([gain_own] * own, axis=0) * (1.0 / (1.0 + jnp.exp(-gate_o)))
    ).astype(BF16)
    heads_own[...] = heads_out

    core = z // half_z
    zl = z % half_z

    @pl.when(tp == core)
    def _():
        heads_all[zl, tp, y] = heads_out

    for d in far_z:
        push(
            heads_own,
            heads_all.at[zl, tp, y],
            hz_send.at[d],
            hz_recv.at[zl, tp],
            z=(z + d) % nz,
            tp=core,
        )

    @pl.when(tp != core)
    def _():
        remote(
            heads_own, heads_all.at[zl, tp, y], hz_send.at[0], hz_recv.at[zl, tp], tp=other
        ).start()

    for k in range(half_z):
        for t in range(2):
            here = heads_all.at[k, t, y]
            source = tp * half_z + k

            @pl.when(jnp.logical_or(source != z, tp != t))
            def _():
                remote(here, here, hz_send.at[0], hz_recv.at[k, t], tp=other).wait_recv()

            for d in near_y:
                push(
                    here, here, hy_send.at[d, k, t], hy_recv.at[y, k, t], y=(y + d) % ny
                )
    for k in range(half_z):
        for t in range(2):
            for d in near_y:
                s = (y + d) % ny
                there = heads_all.at[k, t, s]
                remote(there, there, hy_send.at[d, k, t], hy_recv.at[s, k, t], y=s).wait_recv()
            for s in range(ny):
                start = t * half * heads + (k * ny + s) * piece
                heads_f32[start : start + piece, :] = heads_all[k, t, s].astype(F32)
    gathered = jnp.concatenate(
        [
            heads_f32[pl.ds(t * half * heads + h, half, stride=heads), :].astype(BF16)
            for t in range(2)
            for h in range(heads)
        ],
        axis=1,
    )
    loads[3].wait()
    out_copy.wait_recv()
    attended = jnp.dot(
        gathered, wo_all[...].reshape(2 * heads * 128, 128), preferred_element_type=F32
    )
    mixed = (tok_half[tp].astype(F32) + attended).astype(BF16)
    mixed_all[z, y] = mixed

    for d in far_z:
        push(
            mixed_all.at[z, y], mixed_all.at[z, y], mz_send.at[d], mz_recv.at[z], z=(z + d) % nz
        )
    for d in [0] + near_z:
        s = (z + d) % nz
        here = mixed_all.at[s, y]
        if d:
            remote(here, here, mz_send.at[d], mz_recv.at[s], z=s).wait_recv()
        for e in near_y:
            push(here, here, my_send.at[d, e], my_recv.at[y, s], y=(y + e) % ny)
    loads[4].wait()
    up_copy.wait_recv()
    hidden = up_all.shape[2]
    squares = jnp.zeros((half, 1), F32)
    for d in [0] + near_z:
        s = (z + d) % nz
        for e in near_y:
            src = (y + e) % ny
            there = mixed_all.at[s, src]
            remote(there, there, my_send.at[d, e], my_recv.at[src, s], y=src).wait_recv()
        scaled = []
        for k in range(ny):
            wide_rows = mixed_all[s, k].astype(F32)
            squares = squares + jnp.sum(wide_rows * wide_rows, axis=1, keepdims=True)
            scaled.append((wide_rows * gains[1, pl.ds(s * ny + k, 1), :]).astype(BF16))
        lhs = jnp.concatenate(scaled, axis=1)
        here = pl.ds(pl.multiple_of(s * block, block), block)
        for t in range(2):
            product = jnp.dot(lhs, up_all[t, here, :], preferred_element_type=F32)
            if d:
                product = product + acc[t]
            acc[t] = product
    inverse_mlp = lax.rsqrt(squares / width_full + EPS)
    squared = []
    for t in range(2):
        activation = jnp.maximum(inverse_mlp * acc[t], 0.0)
        squared.append((activation * activation).astype(BF16))

    loads[5].wait()
    down_copy.wait_recv()
    order = far_z + [0]
    for d in order:
        to = (z + d) % nz
        here = pl.ds(pl.multiple_of(to * block, block), block)
        product = jnp.dot(
            squared[0], down_all[0, :, here], preferred_element_type=F32
        ) + jnp.dot(squared[1], down_all[1, :, here], preferred_element_type=F32)
        for k in range(ny):
            down_send[to, k] = product[:, k * 128 : (k + 1) * 128].astype(BF16)
        for e in near_y:
            dst = (y + e) % ny
            push(down_send.at[to, dst], down_y.at[y, to], dy_send.at[d, e], dy_recv.at[y, to], y=dst)
    total = None
    for d in order:
        to = (z + d) % nz
        summed = down_send[to, y].astype(F32)
        for e in near_y:
            src = (y + e) % ny
            there = down_y.at[src, to]
            remote(there, there, dy_send.at[d, e], dy_recv.at[src, to], y=src).wait_recv()
            summed = summed + down_y[src, to].astype(F32)
        if d:
            sum_send[to] = summed.astype(BF16)
            push(sum_send.at[to], sum_recv.at[z], dz_send.at[d], dz_recv.at[z], z=to)
        else:
            total = summed
    for d in near_z:
        s = (z + d) % nz
        remote(sum_recv.at[s], sum_recv.at[s], dz_send.at[d], dz_recv.at[s], z=s).wait_recv()
        total = total + sum_recv[s].astype(F32)
    final = (mixed_all[z, y].astype(F32) + total).astype(BF16)
    fin_send[...] = final
    fin_copy = push(fin_send, fin_recv, pair_send.at[4], pair_recv.at[4], tp=other)
    fin_copy.wait_recv()
    mine, theirs = final.astype(F32), fin_recv[...].astype(F32)
    upper = jnp.where(tp == 0, mine, theirs)
    lower = jnp.where(tp == 0, theirs, mine)
    out[:half] = jnp.where(tp == 0, upper[:, :64], upper[:, 64:]).astype(BF16)
    out[half:] = jnp.where(tp == 0, lower[:, :64], lower[:, 64:]).astype(BF16)

    for copy in pending:
        copy.wait_send()
    for m in range(4):

        @pl.when(y != m)
        def _(m=m):
            remote(weights[m], wbuf.at[y], wy_send.at[m], wy_recv.at[y], y=m).wait_send()

    @pl.when(tp != core)
    def _():
        remote(
            heads_own, heads_all.at[zl, tp, y], hz_send.at[0], hz_recv.at[zl, tp], tp=other
        ).wait_send()


def body(
    tokens,
    gain_mixer,
    weight_query,
    weight_key,
    weight_value,
    weight_outgate,
    weight_ingate,
    weight_forget,
    bias_input,
    bias_forget,
    memory,
    normalizer,
    stabilizer,
    head_gain,
    weight_out,
    gain_channel,
    weight_up,
    weight_down,
):
    nz, ny = lax.axis_size("z"), lax.axis_size("y")
    own, heads, hd = memory.shape[:3]
    width_full = gain_mixer.shape[0]
    rows = tokens.shape[0]
    half = rows // 2
    piece = own * heads
    zrows = ny * own
    block = ny * 128
    dma = pltpu.SemaphoreType.DMA
    vmem = pl.BlockSpec(memory_space=pltpu.VMEM)
    hbm = pl.BlockSpec(memory_space=pl.ANY)
    mem48 = memory.reshape(piece, hd, hd)
    layer_out, inflow_v, key, retain, new_norm, new_stab = pl.pallas_call(
        functools.partial(kernel, nz, ny, width_full),
        out_shape=(
            jax.ShapeDtypeStruct(tokens.shape, BF16),
            jax.ShapeDtypeStruct((piece, hd), F32),
            jax.ShapeDtypeStruct((piece, hd), F32),
            jax.ShapeDtypeStruct((piece, hd), F32),
            jax.ShapeDtypeStruct((piece, hd), F32),
            jax.ShapeDtypeStruct((own, heads), F32),
        ),
        in_specs=[vmem, vmem]
        + [hbm] * 6
        + [vmem, vmem, hbm, vmem, vmem, vmem, hbm, vmem, hbm, hbm],
        out_specs=(vmem,) * 6,
        scratch_shapes=[
            pltpu.VMEM(tokens.shape, BF16),
            pltpu.VMEM((2, half, 128), BF16),
            pltpu.VMEM((ny, rows, 128), BF16),
            pltpu.VMEM((2, width_full // 128, 128), F32),
            pltpu.VMEM((block, 16), BF16),
            pltpu.VMEM((block, 16), BF16),
            pltpu.VMEM((piece, hd, hd), F32),
            pltpu.VMEM((ny, 128, heads, hd), BF16),
            pltpu.VMEM((128 * heads, hd), F32),
            pltpu.VMEM((block, heads * hd), BF16),
            pltpu.VMEM((2, rows, heads * hd // 2), F32),
            pltpu.VMEM((nz, 2 * zrows, heads * hd // 2), BF16),
            pltpu.VMEM((nz, 2 * zrows, heads * hd // 2), BF16),
            pltpu.VMEM((nz, zrows, 128), F32),
            pltpu.VMEM((nz, zrows, 128), F32),
            pltpu.VMEM((zrows * heads, hd), F32),
            pltpu.VMEM((ny, piece, hd), F32),
            pltpu.VMEM((piece, hd), F32),
            pltpu.VMEM((piece, hd), F32),
            pltpu.VMEM((piece, hd), BF16),
            pltpu.VMEM((nz // 2, 2, ny, piece, hd), BF16),
            pltpu.VMEM((2 * half * heads, hd), F32),
            pltpu.VMEM((2, heads * hd, 128), BF16),
            pltpu.VMEM((2, *weight_up.shape), BF16),
            pltpu.VMEM((2, *weight_down.shape), BF16),
            pltpu.VMEM((nz, ny, half, 128), BF16),
            pltpu.VMEM((2, half, weight_up.shape[1]), F32),
            pltpu.VMEM((nz, ny, half, 128), BF16),
            pltpu.VMEM((ny, nz, half, 128), BF16),
            pltpu.VMEM((nz, half, 128), BF16),
            pltpu.VMEM((nz, half, 128), BF16),
            pltpu.VMEM((half, 128), BF16),
            pltpu.VMEM((half, 128), BF16),
            dma((7,)),
            dma((5,)),
            dma((5,)),
            dma((4,)),
            dma((4,)),
            dma((ny,)),
            dma((ny,)),
            dma((nz,)),
            dma((nz,)),
            dma((nz,)),
            dma((nz,)),
            dma((ny,)),
            dma((ny,)),
            dma((nz,)),
            dma((nz // 2, 2)),
            dma((ny, nz // 2, 2)),
            dma((ny, nz // 2, 2)),
            dma((nz,)),
            dma((nz,)),
            dma((nz, ny)),
            dma((ny, nz)),
            dma((nz, ny)),
            dma((ny, nz)),
            dma((nz,)),
            dma((nz,)),
        ],
        compiler_params=pltpu.CompilerParams(
            collective_id=0, has_side_effects=True, vmem_limit_bytes=56 * 1024 * 1024
        ),
    )(
        tokens,
        gain_mixer.reshape(-1, 128),
        weight_query,
        weight_key,
        weight_value,
        weight_outgate,
        weight_ingate,
        weight_forget,
        bias_input.reshape(1, -1),
        bias_forget.reshape(1, -1),
        mem48,
        normalizer.reshape(piece, hd),
        stabilizer,
        head_gain,
        weight_out,
        gain_channel.reshape(-1, 128),
        weight_up,
        weight_down,
    )
    new_memory = (
        retain[:, :1, None] * mem48 + inflow_v[:, :, None] * key[:, None, :]
    ).reshape(memory.shape)
    return (layer_out, new_memory, new_norm.reshape(normalizer.shape), new_stab)


def solution(mesh):
    kv = mesh.shape["kv"]
    ny = 4
    torus = Mesh(
        mesh.devices.reshape(mesh.shape["dp"], kv // ny, ny, mesh.shape["tp"]),
        ("dp", "z", "y", "tp"),
    )
    placed = (
        P("dp", KV_TP),
        P(),
        P(KV, "tp", None),
        P(KV, "tp", None),
        P(KV, "tp", None),
        P(KV, "tp", None),
        P(),
        P(),
        P(),
        P(),
        P(DP_KV, "tp", None, None),
        P(DP_KV, "tp", None),
        P(DP_KV, "tp"),
        P(),
        P("tp", KV),
        P(),
        P(None, KV_TP),
        P(KV_TP, None),
    )
    return jax.shard_map(
        body,
        mesh=torus,
        in_specs=placed,
        out_specs=(
            P("dp", KV_TP),
            P(DP_KV, "tp", None, None),
            P(DP_KV, "tp", None),
            P(DP_KV, "tp"),
        ),
        check_vma=False,
    )
```

time: 291 us -> 104 us (0.36)
  waiting for transfers between devices: 112 us -> 0 us
  Pallas kernels: 0 us -> 90.6 us
  blocking collectives: 73.6 us -> 0 us
  starting transfers between devices: 32.8 us -> 0 us
  matrix products: 16.4 us -> 0 us
  local copies, waits for them, and re-layouts: 25 us -> 9.57 us
  between operations: 14.6 us -> 0.65 us
  other arithmetic: 15.4 us -> 2.92 us
    pallas_call x0 -> x1, Pallas kernels: none -> 90.6 us  [body(): pl.pallas_call(functools.partial(kernel, nz, ny, width_full), out_shape=(...]
    all_to_all x4 -> x0, waiting for transfers between devices: 67.7 us -> none  [the longest x1 48.9 us: sent_and_summed(): lax.all_to_all(tiles, axis, split_axis=0, concat_axis=0, tiled=True)]
    all_gather x3 -> x0, blocking collectives: 46.7 us -> none  [the longest x2 32.6 us: all_blocks(): tiles = lax.all_gather(tiles, axes[k])]
    all_gather x2 -> x0, waiting for transfers between devices: 44.1 us -> none  [the longest x1 23.1 us: whole_of(): nearer = lax.all_gather(value, axes[-1], axis=dim, tiled=True)]
    all_to_all x4 -> x0, starting transfers between devices: 32.7 us -> none  [the longest x2 16.1 us: in_one_piece(): lax.all_to_all(both, axis, split_axis=split_dim, concat_axis=concat_dim,...]
    all_to_all x2 -> x0, blocking collectives: 26.8 us -> none  [the longest x1 15.9 us: sent_to_all(): lax.all_to_all(jnp.broadcast_to(value[None], (count, *value.shape)), axis...]
    dot_general x8 -> x0, matrix products: 16.4 us -> none  [the longest x4 6.63 us: project(): jnp.dot(scaled, weight.reshape(weight.shape[0], -1), preferred_element_ty...]
    reduce_sum x7 -> x0, other arithmetic: 6.83 us -> none  [the longest x2 4.33 us: scale_slab(): jnp.sum(rows_wide * rows_wide, axis=1)]
  transfers between devices with their start and end apart: 6 -> 0, of which waited for: 5 -> 0; matrix products, arithmetic and copies ran while one was open for 4% -> 0% of each run, Pallas kernels for 0% -> 0%
where the time goes in v1:
time: 104 us
  Pallas kernels  90.6 us (87%)
  local copies, waits for them, and re-layouts  9.57 us (9%)
  other arithmetic  2.92 us (3%)
    pallas_call x1, Pallas kernels, body(): pl.pallas_call(functools.partial(kernel, nz, ny, width_full), out_shape=(...  90.6 us
    unnamed x12, local copies, waits for them, and re-layouts  8.65 us
    add x1, other arithmetic, body(): retain[:, :1, None] * mem48 + inflow_v[:, :, None] * key[:, None, :]  2.92 us

profile of v1, /device:TPU:1, one launch (start us, length us, event | category | flops | bytes accessed | tf_op | source)
XLA Modules:
  0.0 103.7 jit_solution(15223441365669295812)
XLA Ops:
  0.6 1.5 %copy.26.tokens = bf16[192,64]{1,0:T(8,128)(2,1)} copy(bf16[192,64]{0,1:T(8,128)(2,1)} %param.18) | data formatting | bytes 49152 | tf_op args[0]
  2.1 2.2 %copy.27.w_in = bf16[4096,16]{1,0:T(8,128)(2,1)} copy(bf16[4096,16]{0,1:T(8,128)(2,1)} %param.24) | data formatting | bytes 262144 | tf_op args[6]
  4.3 2.2 %copy.28.w_forget = bf16[4096,16]{1,0:T(8,128)(2,1)} copy(bf16[4096,16]{0,1:T(8,128)(2,1)} %param.25) | data formatting | bytes 262144 | tf_op args[7]
  6.6 0.0 copy-start
  6.6 90.6 %shard_map.201 = (bf16[192,64]{1,0:T(8,128)(2,1)}, f32[48,128]{1,0:T(8,128)}, f32[48,128]{1,0:T(8,128)}, f32[48,128]{1,0:T(8,128)}, f32[48,128]{1,0:T(8,128)}, /*index=5*/f32[6,8]{1,0:T(8,128)}) custom-call(bf16[192,64]{1,0:T(8,128)(2,1)} %copy.26.tokens, bf16[32,128]{1,0:T(8,128)(2,1)} %bitcast.14, bf16[128,8,128]{2,1,0:T(8,128)(2,1)} %w0.1, ...), custom_call_target="tpu_custom_call" | custom-call | tf_op jit(solution)/shard_map/pallas_call | solution.py:546
  97.1 1.5 %copy.29 = bf16[192,64]{0,1:T(8,128)(2,1)} copy(bf16[192,64]{1,0:T(8,128)(2,1)} %get-tuple-element.20) | data formatting | bytes 49152
  98.6 0.8 slice_reduce_fusion
  99.5 0.1 mul.29
  99.6 0.0 copy-done
  99.6 0.0 copy-start.1
  99.6 0.0 copy-start.2
  99.6 2.9 %multiply_add_fusion = f32[6,8,128,128]{3,2,1,0:T(8,128)} fusion(f32[6,8,128,128]{3,2,1,0:T(8,128)S(1)} %copy-done, f32[6,8,128]{2,1,0:T(8,128)} %bitcast.11, f32[6,8,128]{2,1,0:T(8,128)} %bitcast.10, f32[6,8]{1,0:T(8,128)S(1)} %mul.29), kind=kLoop, calls=%fused_computation | loop fusion | flops 2359296 | bytes 6340800 | tf_op jit(solution)/shard_map/add | solution.py:644
  102.5 0.0 copy-done.1
  102.5 0.6 copy.32
  103.1 0.0 copy-done.2
  103.1 0.6 copy.33
Async XLA Ops:
  6.6 93.0 %copy-start = (f32[6,8,128,128]{3,2,1,0:T(8,128)S(1)}, f32[6,8,128,128]{3,2,1,0:T(8,128)}, u32[]{:S(2)}) copy-start(f32[6,8,128,128]{3,2,1,0:T(8,128)} %param.28) | copy-start | bytes 9437188
  99.6 2.9 %copy-start.1 = (f32[48,128]{1,0:T(8,128)S(1)}, f32[48,128]{1,0:T(8,128)}, u32[]{:S(2)}) copy-start(f32[48,128]{1,0:T(8,128)} %get-tuple-element.14) | copy-start | bytes 73732
  99.6 3.5 %copy-start.2 = (f32[6,8]{1,0:T(8,128)S(1)}, f32[6,8]{1,0:T(8,128)}, u32[]{:S(2)}) copy-start(f32[6,8]{1,0:T(8,128)} %get-tuple-element.31) | copy-start | bytes 580

commit v2 on v1

--- a/solution.py
+++ b/solution.py
@@ -25,30 +25,33 @@
     nz,
     ny,
     width_full,
-    tokens,
-    gain_mixer,
+    tokens_hbm,
+    gain_mixer_hbm,
+    bias_in_hbm,
+    bias_forget_hbm,
+    normalizer_hbm,
+    stabilizer_hbm,
+    head_gain_hbm,
+    gain_channel_hbm,
     w0,
     w1,
     w2,
     w3,
     w_in,
     w_forget,
+    memory,
+    w_out,
+    w_up,
+    w_down,
+    packed,
+    tokens,
+    gain_mixer,
     bias_in,
     bias_forget,
-    memory,
     normalizer,
     stabilizer,
     head_gain,
-    w_out,
     gain_channel,
-    w_up,
-    w_down,
-    out,
-    inflow_v_out,
-    key_out,
-    retain_out,
-    norm_out,
-    stab_out,
     tok_in,
     tok_half,
     tok_all,
@@ -56,17 +59,19 @@
     wig,
     wfg,
     mem,
-    wbuf,
+    mem_split,
+    w_raw,
     wide,
+    w_own,
     w_flat,
-    partial,
     part_send,
     part_recv,
     gate_send,
     gate_recv,
+    rows_wide,
     rows_send,
     rows_recv,
-    q_f32,
+    q_twice,
     mq,
     heads_own,
     heads_all,
@@ -82,6 +87,7 @@
     sum_recv,
     fin_send,
     fin_recv,
+    small_sem,
     local_sem,
     pair_send,
     pair_recv,
@@ -113,7 +119,7 @@
     tp = lax.axis_index("tp")
     other = 1 - tp
     half_z = nz // 2
-    rows = tokens.shape[0]
+    rows = tokens.shape[1]
     half = rows // 2
     own = 6
     heads = 8
@@ -123,6 +129,7 @@
     near_y = by_distance(ny)
     far_z = near_z[::-1]
     pending = []
+    contract = (((1,), (1,)), ((), ()))
 
     def remote(src, dst, send, recv, **to):
         return pltpu.make_async_remote_copy(
@@ -147,43 +154,71 @@
 
     rows_of_block = pl.ds(pl.multiple_of(z * block, block), block)
     loads = [
-        pltpu.make_async_copy(w_in.at[rows_of_block], wig, local_sem.at[0]),
-        pltpu.make_async_copy(w_forget.at[rows_of_block], wfg, local_sem.at[1]),
+        pltpu.make_async_copy(w_in.at[:, rows_of_block], wig, local_sem.at[0]),
+        pltpu.make_async_copy(w_forget.at[:, rows_of_block], wfg, local_sem.at[1]),
         pltpu.make_async_copy(memory, mem, local_sem.at[2]),
         pltpu.make_async_copy(w_out, wo_all.at[tp], local_sem.at[3]),
         pltpu.make_async_copy(w_up, up_all.at[tp], local_sem.at[4]),
         pltpu.make_async_copy(w_down, down_all.at[tp], local_sem.at[5]),
     ]
-    weights = (w0, w1, w2, w3)
+    raw_loads = [
+        pltpu.make_async_copy(w, w_raw.at[m], local_sem.at[6 + m])
+        for m, w in enumerate((w0, w1, w2, w3))
+    ]
+    small = [
+        pltpu.make_async_copy(src, dst, small_sem.at[i])
+        for i, (src, dst) in enumerate(
+            (
+                (tokens_hbm, tokens),
+                (gain_mixer_hbm, gain_mixer),
+                (bias_in_hbm, bias_in),
+                (bias_forget_hbm, bias_forget),
+                (normalizer_hbm, normalizer),
+                (stabilizer_hbm, stabilizer),
+                (head_gain_hbm, head_gain),
+                (gain_channel_hbm, gain_channel),
+            )
+        )
+    ]
+    for copy in raw_loads + small:
+        copy.start()
+    chunks = heads // 2
     for m in range(4):
-
-        @pl.when(y == m)
-        def _(m=m):
-            pltpu.make_async_copy(weights[m], wbuf.at[m], local_sem.at[6]).start()
-
+        raw_loads[m].wait()
+        wide[...] = w_raw[m].astype(F32).reshape(128 * heads, 128)
+        for h in range(heads):
+            w_own[m, h // 2, :, (h % 2) * 128 : (h % 2 + 1) * 128] = wide[
+                pl.ds(h, 128, stride=heads), :
+            ].astype(BF16)
+    for copy in small:
+        copy.wait()
+    gains[0] = gain_mixer[...].astype(F32)
+    gains[1] = gain_channel[...].astype(F32)
+
+    pl.semaphore_wait(barrier, 2 * (nz - 1) + (ny - 1) + 1)
+
+    tok_copy = push(tokens, tok_in, pair_send.at[0], pair_recv.at[0], tp=other)
+    own_block = pl.ds(pl.multiple_of(y * 128, 128), 128)
+
+    def send_chunk(c):
+        for d in near_y:
+            to = (y + d) % ny
+            push(
+                w_own.at[to, c],
+                w_flat.at[c, own_block],
+                wy_send.at[c, d],
+                wy_recv.at[c, y],
+                y=to,
+            )
+
+    send_chunk(0)
     for copy in loads:
         copy.start()
-    gains[0] = gain_mixer[...].astype(F32)
-    gains[1] = gain_channel[...].astype(F32)
-
-    pl.semaphore_wait(barrier, 2 * (nz - 1) + (ny - 1) + 1)
-
-    tok_copy = push(tokens, tok_in, pair_send.at[0], pair_recv.at[0], tp=other)
-    for m in range(4):
-
-        @pl.when(y != m)
-        def _(m=m):
-            remote(weights[m], wbuf.at[y], wy_send.at[m], wy_recv.at[y], y=m).start()
-
-    out_copy = push(w_out, wo_all.at[tp], pair_send.at[1], pair_recv.at[1], tp=other)
-    up_copy = push(w_up, up_all.at[tp], pair_send.at[2], pair_recv.at[2], tp=other)
-    down_copy = push(w_down, down_all.at[tp], pair_send.at[3], pair_recv.at[3], tp=other)
-
     tok_copy.wait_recv()
     mine, theirs = tokens[...].astype(F32), tok_in[...].astype(F32)
     first = jnp.where(tp == 0, mine, theirs)
     second = jnp.where(tp == 0, theirs, mine)
-    chip = jnp.concatenate([first, second], axis=1).astype(BF16)
+    chip = jnp.concatenate([first, second], axis=0).T.astype(BF16)
     tok_all[y] = chip
     tok_half[0] = chip[:half]
     tok_half[1] = chip[half:]
@@ -191,6 +226,13 @@
         push(
             tok_all.at[y], tok_all.at[y], ty_send.at[d], ty_recv.at[y], y=(y + d) % ny
         )
+    for c in range(1, chunks):
+        send_chunk(c)
+    out_copy = push(w_out, wo_all.at[tp], pair_send.at[1], pair_recv.at[1], tp=other)
+    up_copy = push(w_up, up_all.at[tp], pair_send.at[2], pair_recv.at[2], tp=other)
+    down_copy = push(w_down, down_all.at[tp], pair_send.at[3], pair_recv.at[3], tp=other)
+    for c in range(chunks):
+        w_flat[c, own_block] = w_own[y, c]
     for d in near_y:
         s = (y + d) % ny
         remote(tok_all.at[s], tok_all.at[s], ty_send.at[d], ty_recv.at[s], y=s).wait_recv()
@@ -205,8 +247,8 @@
     loads[1].wait()
     gate = jnp.concatenate(
         [
-            jnp.dot(x, wig[...], preferred_element_type=F32),
-            jnp.dot(x, wfg[...], preferred_element_type=F32),
+            lax.dot_general(x, wig[...], contract, preferred_element_type=F32),
+            lax.dot_general(x, wfg[...], contract, preferred_element_type=F32),
             jnp.broadcast_to(squares, (rows, 96)),
         ],
         axis=1,
@@ -217,36 +259,36 @@
         to = (z + d) % nz
         push(gate_send.at[to], gate_recv.at[z], gz_send.at[d], gz_recv.at[z], z=to)
 
-    def flatten(s):
-        wide[...] = wbuf[s].astype(F32).reshape(128 * heads, 128)
-        base = pl.multiple_of(s * 128, 128)
-        for h in range(heads):
-            w_flat[pl.ds(base, 128), h * 128 : (h + 1) * 128] = wide[
-                pl.ds(h, 128, stride=heads), :
-            ].astype(BF16)
-
-    pltpu.make_async_copy(weights[0], wbuf.at[y], local_sem.at[6]).wait()
-    flatten(y)
-    for d in near_y:
-        s = (y + d) % ny
-        remote(wbuf.at[s], wbuf.at[s], wy_send.at[0], wy_recv.at[s], y=s).wait_recv()
-        flatten(s)
-    wcols = heads * 64
-    for n in range(2):
-        partial[n] = jnp.dot(
-            x, w_flat[:, n * wcols : (n + 1) * wcols], preferred_element_type=F32
-        )
-    for k in range(nz):
-        part_send[k] = jnp.concatenate(
-            [
-                partial[0, k * zrows : (k + 1) * zrows, :],
-                partial[1, k * zrows : (k + 1) * zrows, :],
-            ],
-            axis=0,
-        ).astype(BF16)
-    for d in far_z:
-        to = (z + d) % nz
-        push(part_send.at[to], part_recv.at[z], pz_send.at[d], pz_recv.at[z], z=to)
+    for c in range(chunks):
+        for d in near_y:
+            src = (y + d) % ny
+            there = w_flat.at[c, pl.ds(pl.multiple_of(src * 128, 128), 128)]
+            remote(there, there, wy_send.at[c, d], wy_recv.at[c, src], y=src).wait_recv()
+        product = jnp.dot(x, w_flat[c], preferred_element_type=F32)
+        for k in range(nz):
+            part_send[c, k] = jnp.concatenate(
+                [
+                    product[k * zrows : (k + 1) * zrows, :128],
+                    product[k * zrows : (k + 1) * zrows, 128:],
+                ],
+                axis=0,
+            ).astype(BF16)
+        for d in far_z:
+            to = (z + d) % nz
+            push(
+                part_send.at[c, to], part_recv.at[c, z], pz_send.at[c, d], pz_recv.at[c, z], z=to
+            )
+
+    loads[2].wait()
+
+    def split(i, carry):
+        m_bh = mem[i]
+        high = m_bh.astype(BF16)
+        mem_split[i, :, :128] = high
+        mem_split[i, :, 128:] = (m_bh - high.astype(F32)).astype(BF16)
+        return carry
+
+    lax.fori_loop(0, own * heads, split, 0)
 
     gate_sum = gate_send[z]
     for d in near_z:
@@ -265,7 +307,7 @@
     forget = jnp.minimum(forget_pre, 0.0) - jnp.log(1.0 + jnp.exp(-jnp.abs(forget_pre)))
     carried = forget + stabilizer[...]
     new_stab = jnp.maximum(carried, ingate)
-    stab_out[...] = new_stab
+    packed[4 * own * heads : 4 * own * heads + own, :heads] = new_stab
     diagonal = lax.broadcasted_iota(jnp.int32, (heads, heads), 0) == lax.broadcasted_iota(
         jnp.int32, (heads, heads), 1
     )
@@ -287,58 +329,51 @@
     inflow = column(jnp.exp(ingate - new_stab))
     floor = column(jnp.exp(-new_stab))
 
-    total = part_send[z].astype(F32)
-    for d in near_z:
-        s = (z + d) % nz
-        remote(part_recv.at[s], part_recv.at[s], pz_send.at[d], pz_recv.at[s], z=s).wait_recv()
-        total = total + part_recv[s].astype(F32)
-    for h in range(heads):
-        n, c = h // 4, h % 4
-        rows_send[pl.ds(h, zrows, stride=heads), :] = inverse * total[
-            n * zrows : (n + 1) * zrows, c * 128 : (c + 1) * 128
-        ]
+    for c in range(chunks):
+        total = part_send[c, z].astype(F32)
+        for d in near_z:
+            src = (z + d) % nz
+            there = part_recv.at[c, src]
+            remote(there, there, pz_send.at[c, d], pz_recv.at[c, src], z=src).wait_recv()
+            total = total + part_recv[c, src].astype(F32)
+        for i in range(2):
+            rows_wide[pl.ds(2 * c + i, zrows, stride=heads), :] = (
+                inverse * total[i * zrows : (i + 1) * zrows]
+            )
     piece = own * heads
+    for k in range(ny):
+        rows_send[k] = rows_wide[k * piece : (k + 1) * piece, :].astype(BF16)
     for d in near_y:
         to = (y + d) % ny
-        push(
-            rows_send.at[pl.ds(pl.multiple_of(to * piece, piece), piece)],
-            rows_recv.at[y],
-            ry_send.at[d],
-            ry_recv.at[y],
-            y=to,
-        )
-    rows_recv[y] = rows_send[pl.ds(pl.multiple_of(y * piece, piece), piece), :]
+        push(rows_send.at[to], rows_recv.at[y], ry_send.at[d], ry_recv.at[y], y=to)
+    rows_recv[y] = rows_send[y]
     for d in near_y:
         s = (y + d) % ny
         remote(rows_recv.at[s], rows_recv.at[s], ry_send.at[d], ry_recv.at[s], y=s).wait_recv()
 
-    query = rows_recv[0].astype(BF16).astype(F32)
-    key = rows_recv[1].astype(BF16).astype(F32) * 128**-0.5
-    value = rows_recv[2].astype(BF16).astype(F32)
-    gate_o = rows_recv[3].astype(BF16).astype(F32)
-    q_f32[...] = query
+    query = rows_recv[0].astype(F32)
+    key = rows_recv[1].astype(F32) * 128**-0.5
+    value = rows_recv[2].astype(F32)
+    gate_o = rows_recv[3].astype(F32)
+    q_twice[...] = jnp.concatenate([query, query], axis=1)
     new_norm = retain * normalizer[...] + inflow * key
-    norm_out[...] = new_norm
+    packed[3 * piece : 4 * piece] = new_norm
     inflow_value = inflow * value
-    inflow_v_out[...] = inflow_value
-    key_out[...] = key
-    retain_out[...] = jnp.broadcast_to(retain, (piece, 128))
-    loads[2].wait()
+    packed[:piece] = inflow_value
+    packed[piece : 2 * piece] = key
+    packed[2 * piece : 3 * piece] = jnp.broadcast_to(retain, (piece, 128))
     sub = lax.broadcasted_iota(jnp.int32, (heads, 128), 0)
-    contract = (((1,), (1,)), ((), ()))
 
     def readout_of(b, carry):
-        q_b = q_f32[pl.ds(pl.multiple_of(b * heads, heads), heads), :].astype(BF16)
+        here = pl.ds(pl.multiple_of(b * heads, heads), heads)
+        q_b = q_twice[here, :].astype(BF16)
         found = jnp.zeros((heads, 128), F32)
         for h in range(heads):
-            m_bh = mem[b * heads + h]
-            high = m_bh.astype(BF16)
-            low = (m_bh - high.astype(F32)).astype(BF16)
             product = lax.dot_general(
-                q_b, high, contract, preferred_element_type=F32
-            ) + lax.dot_general(q_b, low, contract, preferred_element_type=F32)
+                q_b, mem_split[b * heads + h], contract, preferred_element_type=F32
+            )
             found = jnp.where(sub == h, product, found)
-        mq[pl.ds(pl.multiple_of(b * heads, heads), heads), :] = found
+        mq[here, :] = found
         return carry
 
     lax.fori_loop(0, own, readout_of, 0)
@@ -415,7 +450,7 @@
     mixed = (tok_half[tp].astype(F32) + attended).astype(BF16)
     mixed_all[z, y] = mixed
 
-    for d in far_z:
+    for d in near_z:
         push(
             mixed_all.at[z, y], mixed_all.at[z, y], mz_send.at[d], mz_recv.at[z], z=(z + d) % nz
         )
@@ -491,24 +526,39 @@
     fin_copy = push(fin_send, fin_recv, pair_send.at[4], pair_recv.at[4], tp=other)
     fin_copy.wait_recv()
     mine, theirs = final.astype(F32), fin_recv[...].astype(F32)
-    upper = jnp.where(tp == 0, mine, theirs)
-    lower = jnp.where(tp == 0, theirs, mine)
-    out[:half] = jnp.where(tp == 0, upper[:, :64], upper[:, 64:]).astype(BF16)
-    out[half:] = jnp.where(tp == 0, lower[:, :64], lower[:, 64:]).astype(BF16)
+    top = 4 * piece + 8
+    packed[top : top + half] = jnp.where(tp == 0, mine, theirs)
+    packed[top + half : top + rows] = jnp.where(tp == 0, theirs, mine)
 
     for copy in pending:
         copy.wait_send()
-    for m in range(4):
-
-        @pl.when(y != m)
-        def _(m=m):
-            remote(weights[m], wbuf.at[y], wy_send.at[m], wy_recv.at[y], y=m).wait_send()
-
     @pl.when(tp != core)
     def _():
         remote(
             heads_own, heads_all.at[zl, tp, y], hz_send.at[0], hz_recv.at[zl, tp], tp=other
         ).wait_send()
+
+
+def update(mem, packed, new_mem, out, norm, stab, made, sems):
+    count = sems.shape[0]
+    piece = mem.shape[0]
+    each = piece // count
+    inflow_v = packed[:piece].T
+    copies = []
+    for b in range(count):
+        for i in range(b * each, (b + 1) * each):
+            key, retain = packed[piece + i], packed[2 * piece + i]
+            made[i] = retain[None] * mem[i] + inflow_v[:, i : i + 1] * key[None]
+        here = pl.ds(b * each, each)
+        copies.append(pltpu.make_async_copy(made.at[here], new_mem.at[here], sems.at[b]))
+        copies[-1].start()
+    norm[...] = packed[3 * piece : 4 * piece]
+    stab[...] = packed[4 * piece : 4 * piece + stab.shape[0], : stab.shape[1]]
+    turned = packed[4 * piece + 8 :].T
+    first = lax.axis_index("tp") == 0
+    out[...] = jnp.where(first, turned[:64], turned[64:]).astype(BF16)
+    for copy in copies:
+        copy.wait()
 
 
 def body(
@@ -534,48 +584,54 @@
     nz, ny = lax.axis_size("z"), lax.axis_size("y")
     own, heads, hd = memory.shape[:3]
     width_full = gain_mixer.shape[0]
-    rows = tokens.shape[0]
+    tokens = tokens.T
+    rows = tokens.shape[1]
     half = rows // 2
     piece = own * heads
     zrows = ny * own
     block = ny * 128
+    chunks = heads // 2
     dma = pltpu.SemaphoreType.DMA
     vmem = pl.BlockSpec(memory_space=pltpu.VMEM)
     hbm = pl.BlockSpec(memory_space=pl.ANY)
     mem48 = memory.reshape(piece, hd, hd)
-    layer_out, inflow_v, key, retain, new_norm, new_stab = pl.pallas_call(
+    small = (
+        tokens,
+        gain_mixer.reshape(-1, 128),
+        bias_input.reshape(1, -1),
+        bias_forget.reshape(1, -1),
+        normalizer.reshape(piece, hd),
+        stabilizer,
+        head_gain,
+        gain_channel.reshape(-1, 128),
+    )
+    packed = pl.pallas_call(
         functools.partial(kernel, nz, ny, width_full),
-        out_shape=(
-            jax.ShapeDtypeStruct(tokens.shape, BF16),
-            jax.ShapeDtypeStruct((piece, hd), F32),
-            jax.ShapeDtypeStruct((piece, hd), F32),
-            jax.ShapeDtypeStruct((piece, hd), F32),
-            jax.ShapeDtypeStruct((piece, hd), F32),
-            jax.ShapeDtypeStruct((own, heads), F32),
-        ),
-        in_specs=[vmem, vmem]
-        + [hbm] * 6
-        + [vmem, vmem, hbm, vmem, vmem, vmem, hbm, vmem, hbm, hbm],
-        out_specs=(vmem,) * 6,
-        scratch_shapes=[
+        out_shape=jax.ShapeDtypeStruct((4 * piece + 8 + rows, hd), F32),
+        in_specs=[hbm] * 18,
+        out_specs=vmem,
+        scratch_shapes=[pltpu.VMEM(value.shape, value.dtype) for value in small]
+        + [
             pltpu.VMEM(tokens.shape, BF16),
             pltpu.VMEM((2, half, 128), BF16),
             pltpu.VMEM((ny, rows, 128), BF16),
             pltpu.VMEM((2, width_full // 128, 128), F32),
-            pltpu.VMEM((block, 16), BF16),
-            pltpu.VMEM((block, 16), BF16),
+            pltpu.VMEM((16, block), BF16),
+            pltpu.VMEM((16, block), BF16),
             pltpu.VMEM((piece, hd, hd), F32),
+            pltpu.VMEM((piece, hd, 2 * hd), BF16),
             pltpu.VMEM((ny, 128, heads, hd), BF16),
             pltpu.VMEM((128 * heads, hd), F32),
-            pltpu.VMEM((block, heads * hd), BF16),
-            pltpu.VMEM((2, rows, heads * hd // 2), F32),
-            pltpu.VMEM((nz, 2 * zrows, heads * hd // 2), BF16),
-            pltpu.VMEM((nz, 2 * zrows, heads * hd // 2), BF16),
+            pltpu.VMEM((ny, chunks, 128, 2 * hd), BF16),
+            pltpu.VMEM((chunks, block, 2 * hd), BF16),
+            pltpu.VMEM((chunks, nz, 2 * zrows, hd), BF16),
+            pltpu.VMEM((chunks, nz, 2 * zrows, hd), BF16),
             pltpu.VMEM((nz, zrows, 128), F32),
             pltpu.VMEM((nz, zrows, 128), F32),
             pltpu.VMEM((zrows * heads, hd), F32),
-            pltpu.VMEM((ny, piece, hd), F32),
-            pltpu.VMEM((piece, hd), F32),
+            pltpu.VMEM((ny, piece, hd), BF16),
+            pltpu.VMEM((ny, piece, hd), BF16),
+            pltpu.VMEM((piece, 2 * hd), F32),
             pltpu.VMEM((piece, hd), F32),
             pltpu.VMEM((piece, hd), BF16),
             pltpu.VMEM((nz // 2, 2, ny, piece, hd), BF16),
@@ -591,15 +647,16 @@
             pltpu.VMEM((nz, half, 128), BF16),
             pltpu.VMEM((half, 128), BF16),
             pltpu.VMEM((half, 128), BF16),
-            dma((7,)),
+            dma((8,)),
+            dma((10,)),
             dma((5,)),
             dma((5,)),
-            dma((4,)),
-            dma((4,)),
+            dma((chunks, ny)),
+            dma((chunks, ny)),
             dma((ny,)),
             dma((ny,)),
-            dma((nz,)),
-            dma((nz,)),
+            dma((chunks, nz)),
+            dma((chunks, nz)),
             dma((nz,)),
             dma((nz,)),
             dma((ny,)),
@@ -621,29 +678,33 @@
             collective_id=0, has_side_effects=True, vmem_limit_bytes=56 * 1024 * 1024
         ),
     )(
-        tokens,
-        gain_mixer.reshape(-1, 128),
+        *small,
         weight_query,
         weight_key,
         weight_value,
         weight_outgate,
-        weight_ingate,
-        weight_forget,
-        bias_input.reshape(1, -1),
-        bias_forget.reshape(1, -1),
+        weight_ingate.T,
+        weight_forget.T,
         mem48,
-        normalizer.reshape(piece, hd),
-        stabilizer,
-        head_gain,
         weight_out,
-        gain_channel.reshape(-1, 128),
         weight_up,
         weight_down,
     )
-    new_memory = (
-        retain[:, :1, None] * mem48 + inflow_v[:, :, None] * key[:, None, :]
-    ).reshape(memory.shape)
-    return (layer_out, new_memory, new_norm.reshape(normalizer.shape), new_stab)
+    new_memory, layer_out, new_norm, new_stab = pl.pallas_call(
+        update,
+        out_shape=(
+            jax.ShapeDtypeStruct(mem48.shape, F32),
+            jax.ShapeDtypeStruct(tokens.shape, BF16),
+            jax.ShapeDtypeStruct((piece, hd), F32),
+            jax.ShapeDtypeStruct((own, heads), F32),
+        ),
+        in_specs=[vmem] * 2,
+        out_specs=(hbm, vmem, vmem, vmem),
+        scratch_shapes=[pltpu.VMEM(mem48.shape, F32), dma((own,))],
+        compiler_params=pltpu.CompilerParams(vmem_limit_bytes=16 * 1024 * 1024),
+    )(mem48, packed)
+    new_memory = new_memory.reshape(memory.shape)
+    return (layer_out.T, new_memory, new_norm.reshape(normalizer.shape), new_stab)
 
 
 def solution(mesh):

time: 104 us -> 82.9 us (0.80)
  Pallas kernels: 90.6 us -> 81.2 us
  local copies, waits for them, and re-layouts: 9.57 us -> 0.93 us
  other arithmetic: 2.92 us -> 0 us
    pallas_call x1 -> x2, Pallas kernels: 90.6 us -> 81.2 us  [the longest x1 78.6 us: body(): pl.pallas_call(functools.partial(kernel, nz, ny, width_full), out_shape=j...]
    unnamed x12 -> x4, local copies, waits for them, and re-layouts: 8.65 us -> 0.93 us
    add x1 -> x0, other arithmetic: 2.92 us -> none  [body(): retain[:, :1, None] * mem48 + inflow_v[:, :, None] * key[:, None, :]]
where the time goes in v2:
time: 82.9 us; the launch traced here: 82.8 us
  Pallas kernels  81.2 us (98%)
  local copies, waits for them, and re-layouts  0.93 us (1%)
    pallas_call x1, Pallas kernels, body(): pl.pallas_call(functools.partial(kernel, nz, ny, width_full), out_shape=j...  78.6 us
    pallas_call x1, Pallas kernels, body(): pl.pallas_call(update, out_shape=(jax.ShapeDtypeStruct(mem48.shape, F32),...  2.66 us

profile of v2, /device:TPU:1, one launch (start us, length us, event | category | flops | bytes accessed | tf_op | source)
XLA Modules:
  0.0 82.8 jit_solution(14282934537565165727)
XLA Ops:
  0.6 0.0 copy-start
  0.6 78.6 %shard_map.201.packed = f32[392,128]{1,0:T(8,128)} custom-call(bf16[64,192]{1,0:T(8,128)(2,1)} %bitcast.16, bf16[32,128]{1,0:T(8,128)(2,1)} %bitcast.18, f32[1,16]{1,0:T(1,128)} %bitcast.20, f32[1,16]{1,0:T(1,128)} %bitcast.21, f32[48,128]{1,0:T(8,128)} %bitcast.17, f32[6,8]{1,0:T(8,128)} %stabilizer_hbm.1, bf16[16,128]{1,0:T(8,128)(2,1)} %head_gain_hbm.1, ...), custom_call_target="tpu_custom_call" | custom-call | tf_op jit(solution)/shard_map/pallas_call | solution.py:608
  79.2 0.0 copy-done
  79.2 0.0 copy-start.1
  79.2 0.9 %copy-done.1 = f32[392,128]{1,0:T(8,128)S(1)} copy-done((f32[392,128]{1,0:T(8,128)S(1)}, f32[392,128]{1,0:T(8,128)}, u32[]{:S(2)}) %copy-start.1) | copy-done | bytes 200728
  80.2 2.7 %shard_map.202 = (f32[48,128,128]{2,1,0:T(8,128)}, bf16[64,192]{1,0:T(8,128)(2,1)}, f32[48,128]{1,0:T(8,128)}, f32[6,8]{1,0:T(8,128)}) custom-call(f32[48,128,128]{2,1,0:T(8,128)S(1)} %bitcast.13, f32[392,128]{1,0:T(8,128)S(1)} %copy-done.1), custom_call_target="tpu_custom_call" | custom-call | tf_op jit(solution)/shard_map/pallas_call | solution.py:693
Async XLA Ops:
  0.6 78.6 %copy-start = (f32[6,8,128,128]{3,2,1,0:T(8,128)S(1)}, f32[6,8,128,128]{3,2,1,0:T(8,128)}, u32[]{:S(2)}) copy-start(f32[6,8,128,128]{3,2,1,0:T(8,128)} %param.28) | copy-start | bytes 9437188
  79.2 0.9 %copy-start.1 = (f32[392,128]{1,0:T(8,128)S(1)}, f32[392,128]{1,0:T(8,128)}, u32[]{:S(2)}) copy-start(f32[392,128]{1,0:T(8,128)} %shard_map.201.packed) | copy-start | bytes 602116

commit v3 on v2

--- a/solution.py
+++ b/solution.py
@@ -13,6 +13,7 @@
 KV = ("z", "y")
 DP_KV = ("dp", "z", "y")
 MESH = pl.DeviceIdType.MESH
+PHASES = WY, TY, PZ, GZ, RY, HZ, OY, OX, OP, MZ, MY, DY, DZ = range(13)
 F32 = jnp.float32
 BF16 = jnp.bfloat16
 
@@ -22,6 +23,7 @@
 
 
 def kernel(
+    nx,
     nz,
     ny,
     width_full,
@@ -53,8 +55,8 @@
     head_gain,
     gain_channel,
     tok_in,
-    tok_half,
     tok_all,
+    residual,
     gains,
     wig,
     wfg,
@@ -91,29 +93,15 @@
     local_sem,
     pair_send,
     pair_recv,
-    wy_send,
+    sent,
+    arrived,
     wy_recv,
-    ty_send,
-    ty_recv,
-    pz_send,
     pz_recv,
-    gz_send,
-    gz_recv,
-    ry_send,
-    ry_recv,
-    hz_send,
-    hz_recv,
-    hy_send,
-    hy_recv,
-    mz_send,
     mz_recv,
-    my_send,
     my_recv,
-    dy_send,
     dy_recv,
-    dz_send,
-    dz_recv,
 ):
+    x_rank = lax.axis_index("dp")
     z = lax.axis_index("z")
     y = lax.axis_index("y")
     tp = lax.axis_index("tp")
@@ -127,8 +115,8 @@
     block = ny * 128
     near_z = by_distance(nz)
     near_y = by_distance(ny)
+    near_x = by_distance(nx)
     far_z = near_z[::-1]
-    pending = []
     contract = (((1,), (1,)), ((), ()))
 
     def remote(src, dst, send, recv, **to):
@@ -139,8 +127,13 @@
     def push(*args, **to):
         copy = remote(*args, **to)
         copy.start()
-        pending.append(copy)
         return copy
+
+    def await_sent(ref, sem):
+        remote(ref, ref, sem, sem, tp=other).wait_send()
+
+    def await_all(ref, sem):
+        remote(ref, ref, sem, sem, tp=other).wait_recv()
 
     barrier = pltpu.get_barrier_semaphore()
     for d in near_z:
@@ -150,14 +143,21 @@
             )
     for d in near_y:
         pl.semaphore_signal(barrier, inc=1, device_id={"y": (y + d) % ny}, device_id_type=MESH)
+    for d in near_x:
+        pl.semaphore_signal(barrier, inc=1, device_id={"dp": (x_rank + d) % nx}, device_id_type=MESH)
     pl.semaphore_signal(barrier, inc=1, device_id={"tp": other}, device_id_type=MESH)
+
+    depth = heads * 128
+
+    def out_columns(k):
+        return pl.ds(pl.multiple_of(k * 128, 128), 128)
 
     rows_of_block = pl.ds(pl.multiple_of(z * block, block), block)
     loads = [
         pltpu.make_async_copy(w_in.at[:, rows_of_block], wig, local_sem.at[0]),
         pltpu.make_async_copy(w_forget.at[:, rows_of_block], wfg, local_sem.at[1]),
         pltpu.make_async_copy(memory, mem, local_sem.at[2]),
-        pltpu.make_async_copy(w_out, wo_all.at[tp], local_sem.at[3]),
+        pltpu.make_async_copy(w_out, wo_all.at[tp, :, out_columns(y)], local_sem.at[3]),
         pltpu.make_async_copy(w_up, up_all.at[tp], local_sem.at[4]),
         pltpu.make_async_copy(w_down, down_all.at[tp], local_sem.at[5]),
     ]
@@ -195,7 +195,7 @@
     gains[0] = gain_mixer[...].astype(F32)
     gains[1] = gain_channel[...].astype(F32)
 
-    pl.semaphore_wait(barrier, 2 * (nz - 1) + (ny - 1) + 1)
+    pl.semaphore_wait(barrier, 2 * (nz - 1) + (ny - 1) + (nx - 1) + 1)
 
     tok_copy = push(tokens, tok_in, pair_send.at[0], pair_recv.at[0], tp=other)
     own_block = pl.ds(pl.multiple_of(y * 128, 128), 128)
@@ -206,8 +206,8 @@
             push(
                 w_own.at[to, c],
                 w_flat.at[c, own_block],
-                wy_send.at[c, d],
-                wy_recv.at[c, y],
+                sent.at[WY],
+                wy_recv.at[c],
                 y=to,
             )
 
@@ -220,22 +220,25 @@
     second = jnp.where(tp == 0, theirs, mine)
     chip = jnp.concatenate([first, second], axis=0).T.astype(BF16)
     tok_all[y] = chip
-    tok_half[0] = chip[:half]
-    tok_half[1] = chip[half:]
     for d in near_y:
         push(
-            tok_all.at[y], tok_all.at[y], ty_send.at[d], ty_recv.at[y], y=(y + d) % ny
+            tok_all.at[y], tok_all.at[y], sent.at[TY], arrived.at[TY], y=(y + d) % ny
         )
     for c in range(1, chunks):
         send_chunk(c)
-    out_copy = push(w_out, wo_all.at[tp], pair_send.at[1], pair_recv.at[1], tp=other)
+    share = pl.ds(pl.multiple_of(x_rank * (depth // nx), depth // nx), depth // nx)
+    mine_out = wo_all.at[tp, share, out_columns(y)]
+    for d in near_y:
+        push(
+            w_out.at[share], mine_out, sent.at[OY], arrived.at[OY], y=(y + d) % ny
+        )
+    own_out = wo_all.at[tp, :, out_columns(y)]
+    out_copy = push(w_out, own_out, pair_send.at[1], pair_recv.at[1], tp=other)
     up_copy = push(w_up, up_all.at[tp], pair_send.at[2], pair_recv.at[2], tp=other)
     down_copy = push(w_down, down_all.at[tp], pair_send.at[3], pair_recv.at[3], tp=other)
     for c in range(chunks):
         w_flat[c, own_block] = w_own[y, c]
-    for d in near_y:
-        s = (y + d) % ny
-        remote(tok_all.at[s], tok_all.at[s], ty_send.at[d], ty_recv.at[s], y=s).wait_recv()
+    await_all(tok_all.at[: ny - 1], arrived.at[TY])
     squares = jnp.zeros((rows, 1), F32)
     scaled = []
     for s in range(ny):
@@ -257,13 +260,10 @@
         gate_send[k] = gate[k * zrows : (k + 1) * zrows]
     for d in far_z:
         to = (z + d) % nz
-        push(gate_send.at[to], gate_recv.at[z], gz_send.at[d], gz_recv.at[z], z=to)
+        push(gate_send.at[to], gate_recv.at[z], sent.at[GZ], arrived.at[GZ], z=to)
 
     for c in range(chunks):
-        for d in near_y:
-            src = (y + d) % ny
-            there = w_flat.at[c, pl.ds(pl.multiple_of(src * 128, 128), 128)]
-            remote(there, there, wy_send.at[c, d], wy_recv.at[c, src], y=src).wait_recv()
+        await_all(w_flat.at[c, : (ny - 1) * 128], wy_recv.at[c])
         product = jnp.dot(x, w_flat[c], preferred_element_type=F32)
         for k in range(nz):
             part_send[c, k] = jnp.concatenate(
@@ -276,7 +276,7 @@
         for d in far_z:
             to = (z + d) % nz
             push(
-                part_send.at[c, to], part_recv.at[c, z], pz_send.at[c, d], pz_recv.at[c, z], z=to
+                part_send.at[c, to], part_recv.at[c, z], sent.at[PZ], pz_recv.at[c], z=to
             )
 
     loads[2].wait()
@@ -290,11 +290,23 @@
 
     lax.fori_loop(0, own * heads, split, 0)
 
+    at = lax.broadcasted_iota(jnp.int32, (half_z * own, rows), 0)
+    row = at + tp * half + y * own
+    for k in range(1, half_z):
+        row = row + jnp.where(at >= k * own, zrows - own, 0)
+    chosen = jnp.where(
+        lax.broadcasted_iota(jnp.int32, (half_z * own, rows), 1) == row, 1.0, 0.0
+    ).astype(BF16)
+    residual[...] = jnp.dot(
+        chosen,
+        jnp.concatenate([tok_all[k] for k in range(ny)], axis=1),
+        preferred_element_type=F32,
+    )
+
+    await_all(gate_recv.at[: nz - 1], arrived.at[GZ])
     gate_sum = gate_send[z]
     for d in near_z:
-        s = (z + d) % nz
-        remote(gate_recv.at[s], gate_recv.at[s], gz_send.at[d], gz_recv.at[s], z=s).wait_recv()
-        gate_sum = gate_sum + gate_recv[s]
+        gate_sum = gate_sum + gate_recv[(z + d) % nz]
     inverse = lax.rsqrt(gate_sum[:, 32:33] / width_full + EPS)
     gate_pre = inverse * gate_sum
     gate_rows = jnp.zeros((own, 128), F32)
@@ -330,11 +342,16 @@
     floor = column(jnp.exp(-new_stab))
 
     for c in range(chunks):
+        if c == chunks - 1:
+            await_all(wo_all.at[tp, share, : (ny - 1) * 128], arrived.at[OY])
+            for d in near_y:
+                there = wo_all.at[tp, share, out_columns((y + d) % ny)]
+                for e in near_x:
+                    push(there, there, sent.at[OX], arrived.at[OX], dp=(x_rank + e) % nx)
+        await_all(part_recv.at[c, : nz - 1], pz_recv.at[c])
         total = part_send[c, z].astype(F32)
         for d in near_z:
             src = (z + d) % nz
-            there = part_recv.at[c, src]
-            remote(there, there, pz_send.at[c, d], pz_recv.at[c, src], z=src).wait_recv()
             total = total + part_recv[c, src].astype(F32)
         for i in range(2):
             rows_wide[pl.ds(2 * c + i, zrows, stride=heads), :] = (
@@ -345,11 +362,9 @@
         rows_send[k] = rows_wide[k * piece : (k + 1) * piece, :].astype(BF16)
     for d in near_y:
         to = (y + d) % ny
-        push(rows_send.at[to], rows_recv.at[y], ry_send.at[d], ry_recv.at[y], y=to)
+        push(rows_send.at[to], rows_recv.at[y], sent.at[RY], arrived.at[RY], y=to)
     rows_recv[y] = rows_send[y]
-    for d in near_y:
-        s = (y + d) % ny
-        remote(rows_recv.at[s], rows_recv.at[s], ry_send.at[d], ry_recv.at[s], y=s).wait_recv()
+    await_all(rows_recv.at[: ny - 1], arrived.at[RY])
 
     query = rows_recv[0].astype(F32)
     key = rows_recv[1].astype(F32) * 128**-0.5
@@ -394,96 +409,93 @@
 
     @pl.when(tp == core)
     def _():
-        heads_all[zl, tp, y] = heads_out
+        heads_all[2 * zl + tp] = heads_out
 
     for d in far_z:
         push(
             heads_own,
-            heads_all.at[zl, tp, y],
-            hz_send.at[d],
-            hz_recv.at[zl, tp],
+            heads_all.at[2 * zl + tp],
+            sent.at[HZ],
+            arrived.at[HZ],
             z=(z + d) % nz,
             tp=core,
         )
 
     @pl.when(tp != core)
     def _():
-        remote(
-            heads_own, heads_all.at[zl, tp, y], hz_send.at[0], hz_recv.at[zl, tp], tp=other
-        ).start()
+        push(heads_own, heads_all.at[2 * zl + tp], sent.at[HZ], arrived.at[HZ], tp=other)
+
+    loads[3].wait()
+    if nx > 1:
+        passed_on = wo_all.at[tp, : depth // nx * (nx - 1), : (ny - 1) * 128]
+        await_all(passed_on, arrived.at[OX])
+    for d in near_y:
+        whole = wo_all.at[tp, :, out_columns((y + d) % ny)]
+        push(whole, whole, sent.at[OP], arrived.at[OP], tp=other)
+
+    @pl.when(tp == core)
+    def _():
+        await_all(heads_all.at[: nz - 1], arrived.at[HZ])
+
+    @pl.when(tp != core)
+    def _():
+        await_all(heads_all, arrived.at[HZ])
 
     for k in range(half_z):
         for t in range(2):
-            here = heads_all.at[k, t, y]
-            source = tp * half_z + k
-
-            @pl.when(jnp.logical_or(source != z, tp != t))
-            def _():
-                remote(here, here, hz_send.at[0], hz_recv.at[k, t], tp=other).wait_recv()
-
-            for d in near_y:
-                push(
-                    here, here, hy_send.at[d, k, t], hy_recv.at[y, k, t], y=(y + d) % ny
-                )
-    for k in range(half_z):
-        for t in range(2):
-            for d in near_y:
-                s = (y + d) % ny
-                there = heads_all.at[k, t, s]
-                remote(there, there, hy_send.at[d, k, t], hy_recv.at[s, k, t], y=s).wait_recv()
-            for s in range(ny):
-                start = t * half * heads + (k * ny + s) * piece
-                heads_f32[start : start + piece, :] = heads_all[k, t, s].astype(F32)
+            start = (t * half_z + k) * piece
+            heads_f32[start : start + piece, :] = heads_all[2 * k + t].astype(F32)
+    mrows = half_z * own
     gathered = jnp.concatenate(
         [
-            heads_f32[pl.ds(t * half * heads + h, half, stride=heads), :].astype(BF16)
+            heads_f32[pl.ds(t * half_z * piece + h, mrows, stride=heads), :].astype(BF16)
             for t in range(2)
             for h in range(heads)
         ],
         axis=1,
     )
-    loads[3].wait()
     out_copy.wait_recv()
+    await_all(wo_all.at[other, :, : (ny - 1) * 128], arrived.at[OP])
     attended = jnp.dot(
-        gathered, wo_all[...].reshape(2 * heads * 128, 128), preferred_element_type=F32
-    )
-    mixed = (tok_half[tp].astype(F32) + attended).astype(BF16)
-    mixed_all[z, y] = mixed
+        gathered, wo_all[...].reshape(2 * depth, block), preferred_element_type=F32
+    )
+    mixed = residual[...] + attended
+    wcols = block // 2
+    mixed_all[z, y] = jnp.concatenate([mixed[:, :wcols], mixed[:, wcols:]], axis=0).astype(BF16)
 
     for d in near_z:
         push(
-            mixed_all.at[z, y], mixed_all.at[z, y], mz_send.at[d], mz_recv.at[z], z=(z + d) % nz
+            mixed_all.at[z, y], mixed_all.at[z, y], sent.at[MZ], mz_recv.at[z], z=(z + d) % nz
         )
     for d in [0] + near_z:
         s = (z + d) % nz
         here = mixed_all.at[s, y]
         if d:
-            remote(here, here, mz_send.at[d], mz_recv.at[s], z=s).wait_recv()
+            await_all(here, mz_recv.at[s])
         for e in near_y:
-            push(here, here, my_send.at[d, e], my_recv.at[y, s], y=(y + e) % ny)
+            push(here, here, sent.at[MY], my_recv.at[s], y=(y + e) % ny)
     loads[4].wait()
     up_copy.wait_recv()
     hidden = up_all.shape[2]
-    squares = jnp.zeros((half, 1), F32)
+    squares = [jnp.zeros((mrows, 1), F32)] * ny
     for d in [0] + near_z:
         s = (z + d) % nz
-        for e in near_y:
-            src = (y + e) % ny
-            there = mixed_all.at[s, src]
-            remote(there, there, my_send.at[d, e], my_recv.at[src, s], y=src).wait_recv()
+        await_all(mixed_all.at[s, : ny - 1], my_recv.at[s])
+        gain = jnp.concatenate([gains[1, pl.ds(s * ny + k, 1), :] for k in range(ny)], axis=1)
         scaled = []
         for k in range(ny):
-            wide_rows = mixed_all[s, k].astype(F32)
-            squares = squares + jnp.sum(wide_rows * wide_rows, axis=1, keepdims=True)
-            scaled.append((wide_rows * gains[1, pl.ds(s * ny + k, 1), :]).astype(BF16))
-        lhs = jnp.concatenate(scaled, axis=1)
+            stacked = mixed_all[s, k].astype(F32)
+            wide_rows = jnp.concatenate([stacked[:mrows], stacked[mrows:]], axis=1)
+            squares[k] = squares[k] + jnp.sum(wide_rows * wide_rows, axis=1, keepdims=True)
+            scaled.append(wide_rows * gain)
+        lhs = jnp.concatenate(scaled, axis=0).astype(BF16)
         here = pl.ds(pl.multiple_of(s * block, block), block)
         for t in range(2):
             product = jnp.dot(lhs, up_all[t, here, :], preferred_element_type=F32)
             if d:
                 product = product + acc[t]
             acc[t] = product
-    inverse_mlp = lax.rsqrt(squares / width_full + EPS)
+    inverse_mlp = lax.rsqrt(jnp.concatenate(squares, axis=0) / width_full + EPS)
     squared = []
     for t in range(2):
         activation = jnp.maximum(inverse_mlp * acc[t], 0.0)
@@ -502,44 +514,78 @@
             down_send[to, k] = product[:, k * 128 : (k + 1) * 128].astype(BF16)
         for e in near_y:
             dst = (y + e) % ny
-            push(down_send.at[to, dst], down_y.at[y, to], dy_send.at[d, e], dy_recv.at[y, to], y=dst)
-    total = None
+            push(down_send.at[to, dst], down_y.at[y, to], sent.at[DY], dy_recv.at[to], y=dst)
+    quarter = half // 2
+
+    def columns_of(value, t):
+        cols = value[:, 64 * t : 64 * (t + 1)]
+        return jnp.concatenate([cols[:quarter], cols[quarter:]], axis=1)
+
     for d in order:
         to = (z + d) % nz
+        await_all(down_y.at[: ny - 1, to], dy_recv.at[to])
         summed = down_send[to, y].astype(F32)
         for e in near_y:
-            src = (y + e) % ny
-            there = down_y.at[src, to]
-            remote(there, there, dy_send.at[d, e], dy_recv.at[src, to], y=src).wait_recv()
-            summed = summed + down_y[src, to].astype(F32)
+            summed = summed + down_y[(y + e) % ny, to].astype(F32)
         if d:
-            sum_send[to] = summed.astype(BF16)
-            push(sum_send.at[to], sum_recv.at[z], dz_send.at[d], dz_recv.at[z], z=to)
+            for t in range(2):
+                sum_send[t, to] = columns_of(summed, t).astype(BF16)
+                push(sum_send.at[t, to], sum_recv.at[tp, z], sent.at[DZ], arrived.at[DZ], z=to, tp=t)
         else:
-            total = summed
+            carried = []
+            for k in range(ny):
+                stacked = mixed_all[z, k].astype(F32)
+                mine = jnp.zeros((mrows, 128), F32)
+                for c in range(ny):
+                    down, across = c // (ny // 2) * mrows, c % (ny // 2) * 128
+                    mine = jnp.where(
+                        y == c, stacked[down : down + mrows, across : across + 128], mine
+                    )
+                carried.append(mine)
+            whole = summed + jnp.concatenate(carried, axis=0)
+            fin_send[0] = columns_of(whole, 0)
+            fin_send[1] = columns_of(whole, 1)
+            fin_copy = push(
+                fin_send.at[other], fin_recv, pair_send.at[4], pair_recv.at[4], tp=other
+            )
+    await_all(sum_recv.at[:, : nz - 1], arrived.at[DZ])
+    total = [fin_send[tp], jnp.zeros((quarter, 128), F32)]
     for d in near_z:
-        s = (z + d) % nz
-        remote(sum_recv.at[s], sum_recv.at[s], dz_send.at[d], dz_recv.at[s], z=s).wait_recv()
-        total = total + sum_recv[s].astype(F32)
-    final = (mixed_all[z, y].astype(F32) + total).astype(BF16)
-    fin_send[...] = final
-    fin_copy = push(fin_send, fin_recv, pair_send.at[4], pair_recv.at[4], tp=other)
+        src = (z + d) % nz
+        total[0] = total[0] + sum_recv[tp, src].astype(F32)
+        total[1] = total[1] + sum_recv[other, src].astype(F32)
     fin_copy.wait_recv()
-    mine, theirs = final.astype(F32), fin_recv[...].astype(F32)
+    total[1] = total[1] + fin_recv[...]
     top = 4 * piece + 8
-    packed[top : top + half] = jnp.where(tp == 0, mine, theirs)
-    packed[top + half : top + rows] = jnp.where(tp == 0, theirs, mine)
-
-    for copy in pending:
+    packed[top : top + quarter] = jnp.where(tp == 0, total[0], total[1])
+    packed[top + quarter : top + half] = jnp.where(tp == 0, total[1], total[0])
+
+    for copy in (tok_copy, out_copy, up_copy, down_copy, fin_copy):
         copy.wait_send()
+    await_sent(w_own.at[: ny - 1], sent.at[WY])
+    await_sent(tok_all.at[: ny - 1], sent.at[TY])
+    await_sent(part_send.at[:, : nz - 1], sent.at[PZ])
+    await_sent(gate_send.at[: nz - 1], sent.at[GZ])
+    await_sent(rows_send.at[: ny - 1], sent.at[RY])
+    await_sent(wo_all.at[tp, share, : (ny - 1) * 128], sent.at[OY])
+    if nx > 1:
+        await_sent(passed_on, sent.at[OX])
+    await_sent(wo_all.at[tp, :, : (ny - 1) * 128], sent.at[OP])
+    await_sent(mixed_all.at[: nz - 1, 0], sent.at[MZ])
+    await_sent(mixed_all.at[:, : ny - 1], sent.at[MY])
+    await_sent(down_send.at[:, : ny - 1], sent.at[DY])
+    await_sent(sum_send.at[:, : nz - 1], sent.at[DZ])
+
+    @pl.when(tp == core)
+    def _():
+        await_sent(heads_all.at[: nz - 1], sent.at[HZ])
+
     @pl.when(tp != core)
     def _():
-        remote(
-            heads_own, heads_all.at[zl, tp, y], hz_send.at[0], hz_recv.at[zl, tp], tp=other
-        ).wait_send()
-
-
-def update(mem, packed, new_mem, out, norm, stab, made, sems):
+        await_sent(heads_all, sent.at[HZ])
+
+
+def update(ny, mem, packed, new_mem, out, norm, stab, made, sems):
     count = sems.shape[0]
     piece = mem.shape[0]
     each = piece // count
@@ -554,9 +600,27 @@
         copies[-1].start()
     norm[...] = packed[3 * piece : 4 * piece]
     stab[...] = packed[4 * piece : 4 * piece + stab.shape[0], : stab.shape[1]]
-    turned = packed[4 * piece + 8 :].T
-    first = lax.axis_index("tp") == 0
-    out[...] = jnp.where(first, turned[:64], turned[64:]).astype(BF16)
+    rows = out.shape[1]
+    own, blocks = stab.shape[0], rows // stab.shape[0] // 2
+    per = blocks // ny
+    quarter = rows // 4
+    line = lax.broadcasted_iota(jnp.int32, (rows // 2, rows), 0).astype(F32)
+    column = lax.broadcasted_iota(jnp.int32, (rows // 2, rows), 1).astype(F32)
+    side = jnp.where(line >= quarter, 1.0, 0.0)
+    result = packed[4 * piece + 8 :].T.astype(BF16)
+    turned = jnp.zeros((64, rows), F32)
+    for upper in range(2):
+        at = line + side * quarter + upper * quarter
+        group = jnp.floor((at + 0.5) / own)
+        inner = group - side * blocks
+        in_y = jnp.floor((inner + 0.5) / per)
+        in_z = inner - in_y * per
+        target = (side * blocks + in_z * ny + in_y) * own + (at - group * own)
+        order = jnp.where(column == target, 1.0, 0.0).astype(BF16)
+        turned = turned + jnp.dot(
+            result[64 * upper : 64 * (upper + 1)], order, preferred_element_type=F32
+        )
+    out[...] = turned.astype(BF16)
     for copy in copies:
         copy.wait()
 
@@ -581,7 +645,7 @@
     weight_up,
     weight_down,
 ):
-    nz, ny = lax.axis_size("z"), lax.axis_size("y")
+    nx, nz, ny = lax.axis_size("dp"), lax.axis_size("z"), lax.axis_size("y")
     own, heads, hd = memory.shape[:3]
     width_full = gain_mixer.shape[0]
     tokens = tokens.T
@@ -591,6 +655,7 @@
     zrows = ny * own
     block = ny * 128
     chunks = heads // 2
+    mrows = nz // 2 * own
     dma = pltpu.SemaphoreType.DMA
     vmem = pl.BlockSpec(memory_space=pltpu.VMEM)
     hbm = pl.BlockSpec(memory_space=pl.ANY)
@@ -606,15 +671,15 @@
         gain_channel.reshape(-1, 128),
     )
     packed = pl.pallas_call(
-        functools.partial(kernel, nz, ny, width_full),
-        out_shape=jax.ShapeDtypeStruct((4 * piece + 8 + rows, hd), F32),
+        functools.partial(kernel, nx, nz, ny, width_full),
+        out_shape=jax.ShapeDtypeStruct((4 * piece + 8 + half, hd), F32),
         in_specs=[hbm] * 18,
         out_specs=vmem,
         scratch_shapes=[pltpu.VMEM(value.shape, value.dtype) for value in small]
         + [
             pltpu.VMEM(tokens.shape, BF16),
-            pltpu.VMEM((2, half, 128), BF16),
             pltpu.VMEM((ny, rows, 128), BF16),
+            pltpu.VMEM((mrows, block), F32),
             pltpu.VMEM((2, width_full // 128, 128), F32),
             pltpu.VMEM((16, block), BF16),
             pltpu.VMEM((16, block), BF16),
@@ -634,43 +699,28 @@
             pltpu.VMEM((piece, 2 * hd), F32),
             pltpu.VMEM((piece, hd), F32),
             pltpu.VMEM((piece, hd), BF16),
-            pltpu.VMEM((nz // 2, 2, ny, piece, hd), BF16),
-            pltpu.VMEM((2 * half * heads, hd), F32),
-            pltpu.VMEM((2, heads * hd, 128), BF16),
+            pltpu.VMEM((nz, piece, hd), BF16),
+            pltpu.VMEM((nz * piece, hd), F32),
+            pltpu.VMEM((2, heads * hd, block), BF16),
             pltpu.VMEM((2, *weight_up.shape), BF16),
             pltpu.VMEM((2, *weight_down.shape), BF16),
-            pltpu.VMEM((nz, ny, half, 128), BF16),
+            pltpu.VMEM((nz, ny, 2 * mrows, block // 2), BF16),
             pltpu.VMEM((2, half, weight_up.shape[1]), F32),
             pltpu.VMEM((nz, ny, half, 128), BF16),
             pltpu.VMEM((ny, nz, half, 128), BF16),
-            pltpu.VMEM((nz, half, 128), BF16),
-            pltpu.VMEM((nz, half, 128), BF16),
-            pltpu.VMEM((half, 128), BF16),
-            pltpu.VMEM((half, 128), BF16),
+            pltpu.VMEM((2, nz, half // 2, 128), BF16),
+            pltpu.VMEM((2, nz, half // 2, 128), BF16),
+            pltpu.VMEM((2, half // 2, 128), F32),
+            pltpu.VMEM((half // 2, 128), F32),
             dma((8,)),
             dma((10,)),
             dma((5,)),
             dma((5,)),
-            dma((chunks, ny)),
-            dma((chunks, ny)),
-            dma((ny,)),
-            dma((ny,)),
-            dma((chunks, nz)),
-            dma((chunks, nz)),
+            dma((len(PHASES),)),
+            dma((len(PHASES),)),
+            dma((chunks,)),
+            dma((chunks,)),
             dma((nz,)),
-            dma((nz,)),
-            dma((ny,)),
-            dma((ny,)),
-            dma((nz,)),
-            dma((nz // 2, 2)),
-            dma((ny, nz // 2, 2)),
-            dma((ny, nz // 2, 2)),
-            dma((nz,)),
-            dma((nz,)),
-            dma((nz, ny)),
-            dma((ny, nz)),
-            dma((nz, ny)),
-            dma((ny, nz)),
             dma((nz,)),
             dma((nz,)),
         ],
@@ -691,7 +741,7 @@
         weight_down,
     )
     new_memory, layer_out, new_norm, new_stab = pl.pallas_call(
-        update,
+        functools.partial(update, ny),
         out_shape=(
             jax.ShapeDtypeStruct(mem48.shape, F32),
             jax.ShapeDtypeStruct(tokens.shape, BF16),

time: 82.9 us -> 74.8 us (0.902)
  Pallas kernels: 81.2 us -> 73.1 us
    pallas_call x2, Pallas kernels: 81.2 us -> 73.1 us  [the longest x1 70.4 us: body(): pl.pallas_call(functools.partial(kernel, nx, nz, ny, width_full), out_sha...]
where the time goes in v3:
time: 74.8 us; the launch traced here: 74.7 us
  Pallas kernels  73.1 us (98%)
  local copies, waits for them, and re-layouts  0.91 us (1%)
    pallas_call x1, Pallas kernels, body(): pl.pallas_call(functools.partial(kernel, nx, nz, ny, width_full), out_sha...  70.4 us
    pallas_call x1, Pallas kernels, body(): pl.pallas_call(functools.partial(update, ny), out_shape=(jax.ShapeDtypeSt...  2.67 us

profile of v3, /device:TPU:1, one launch (start us, length us, event | category | flops | bytes accessed | tf_op | source)
XLA Modules:
  0.0 74.7 jit_solution(17601196867953715995)
XLA Ops:
  0.6 0.0 copy-start
  0.6 70.4 %shard_map.201.packed = f32[296,128]{1,0:T(8,128)} custom-call(bf16[64,192]{1,0:T(8,128)(2,1)} %bitcast.16, bf16[32,128]{1,0:T(8,128)(2,1)} %bitcast.18, f32[1,16]{1,0:T(1,128)} %bitcast.20, f32[1,16]{1,0:T(1,128)} %bitcast.21, f32[48,128]{1,0:T(8,128)} %bitcast.17, f32[6,8]{1,0:T(8,128)} %stabilizer_hbm.1, bf16[16,128]{1,0:T(8,128)(2,1)} %head_gain_hbm.1, ...), custom_call_target="tpu_custom_call" | custom-call | tf_op jit(solution)/shard_map/pallas_call | solution.py:673
  71.1 0.0 copy-done
  71.1 0.0 copy-start.1
  71.1 0.9 %copy-done.1 = f32[296,128]{1,0:T(8,128)S(1)} copy-done((f32[296,128]{1,0:T(8,128)S(1)}, f32[296,128]{1,0:T(8,128)}, u32[]{:S(2)}) %copy-start.1) | copy-done | bytes 151576
  72.0 2.7 %shard_map.202 = (f32[48,128,128]{2,1,0:T(8,128)}, bf16[64,192]{1,0:T(8,128)(2,1)}, f32[48,128]{1,0:T(8,128)}, f32[6,8]{1,0:T(8,128)}) custom-call(f32[48,128,128]{2,1,0:T(8,128)S(1)} %bitcast.13, f32[296,128]{1,0:T(8,128)S(1)} %copy-done.1), custom_call_target="tpu_custom_call" | custom-call | tf_op jit(solution)/shard_map/pallas_call | solution.py:743
Async XLA Ops:
  0.6 70.4 %copy-start = (f32[6,8,128,128]{3,2,1,0:T(8,128)S(1)}, f32[6,8,128,128]{3,2,1,0:T(8,128)}, u32[]{:S(2)}) copy-start(f32[6,8,128,128]{3,2,1,0:T(8,128)} %param.28) | copy-start | bytes 9437188
  71.1 0.9 %copy-start.1 = (f32[296,128]{1,0:T(8,128)S(1)}, f32[296,128]{1,0:T(8,128)}, u32[]{:S(2)}) copy-start(f32[296,128]{1,0:T(8,128)} %shard_map.201.packed) | copy-start | bytes 454660

commit v4 on v3

--- a/solution.py
+++ b/solution.py
@@ -13,7 +13,7 @@
 KV = ("z", "y")
 DP_KV = ("dp", "z", "y")
 MESH = pl.DeviceIdType.MESH
-PHASES = WY, TY, PZ, GZ, RY, HZ, OY, OX, OP, MZ, MY, DY, DZ = range(13)
+PHASES = WY, WQ, WX, TY, PZ, GZ, RY, HZ, OY, OX, OD, OP, MZ, MN, MY, DN, DY, DZ = range(18)
 F32 = jnp.float32
 BF16 = jnp.bfloat16
 
@@ -84,6 +84,8 @@
     mixed_all,
     acc,
     down_send,
+    down_own,
+    down_next,
     down_y,
     sum_send,
     sum_recv,
@@ -117,6 +119,8 @@
     near_y = by_distance(ny)
     near_x = by_distance(nx)
     far_z = near_z[::-1]
+    next_z = [d for d in near_z if min(d, nz - d) == 1]
+    rest_z = [d for d in near_z if d not in next_z]
     contract = (((1,), (1,)), ((), ()))
 
     def remote(src, dst, send, recv, **to):
@@ -211,7 +215,22 @@
                 y=to,
             )
 
+    last = chunks - 1
+    some = 128 // nx
+
+    def share_of(k):
+        return pl.ds(pl.multiple_of(k * 128 + x_rank * some, some), some)
+
     send_chunk(0)
+    for d in near_y:
+        to = (y + d) % ny
+        push(
+            w_own.at[to, last, share_of(0)],
+            w_flat.at[last, share_of(y)],
+            sent.at[WQ],
+            arrived.at[WQ],
+            y=to,
+        )
     for copy in loads:
         copy.start()
     tok_copy.wait_recv()
@@ -224,46 +243,37 @@
         push(
             tok_all.at[y], tok_all.at[y], sent.at[TY], arrived.at[TY], y=(y + d) % ny
         )
-    for c in range(1, chunks):
+    for c in range(1, last):
         send_chunk(c)
-    share = pl.ds(pl.multiple_of(x_rank * (depth // nx), depth // nx), depth // nx)
-    mine_out = wo_all.at[tp, share, out_columns(y)]
+    direct = depth // 2
+    part = (depth - direct) // nx
+    share = pl.ds(pl.multiple_of(direct + x_rank * part, part), part)
     for d in near_y:
-        push(
-            w_out.at[share], mine_out, sent.at[OY], arrived.at[OY], y=(y + d) % ny
-        )
+        to = (y + d) % ny
+        push(w_out.at[share], wo_all.at[tp, share, out_columns(y)], sent.at[OY], arrived.at[OY], y=to)
+    head = pl.ds(0, direct)
+    for d in near_y:
+        to = (y + d) % ny
+        push(w_out.at[head], wo_all.at[tp, head, out_columns(y)], sent.at[OD], arrived.at[OD], y=to)
     own_out = wo_all.at[tp, :, out_columns(y)]
     out_copy = push(w_out, own_out, pair_send.at[1], pair_recv.at[1], tp=other)
-    up_copy = push(w_up, up_all.at[tp], pair_send.at[2], pair_recv.at[2], tp=other)
-    down_copy = push(w_down, down_all.at[tp], pair_send.at[3], pair_recv.at[3], tp=other)
     for c in range(chunks):
         w_flat[c, own_block] = w_own[y, c]
+    await_all(w_flat.at[last, : (ny - 1) * some], arrived.at[WQ])
+    for d in near_y:
+        there = w_flat.at[last, share_of((y + d) % ny)]
+        for e in near_x:
+            push(there, there, sent.at[WX], arrived.at[WX], dp=(x_rank + e) % nx)
     await_all(tok_all.at[: ny - 1], arrived.at[TY])
-    squares = jnp.zeros((rows, 1), F32)
-    scaled = []
-    for s in range(ny):
-        wide_rows = tok_all[s].astype(F32)
-        squares = squares + jnp.sum(wide_rows * wide_rows, axis=1, keepdims=True)
-        scaled.append((wide_rows * gains[0, pl.ds(z * ny + s, 1), :]).astype(BF16))
-    x = jnp.concatenate(scaled, axis=1)
-    loads[0].wait()
-    loads[1].wait()
-    gate = jnp.concatenate(
+    x = jnp.concatenate(
         [
-            lax.dot_general(x, wig[...], contract, preferred_element_type=F32),
-            lax.dot_general(x, wfg[...], contract, preferred_element_type=F32),
-            jnp.broadcast_to(squares, (rows, 96)),
+            (tok_all[s].astype(F32) * gains[0, pl.ds(z * ny + s, 1), :]).astype(BF16)
+            for s in range(ny)
         ],
         axis=1,
     )
-    for k in range(nz):
-        gate_send[k] = gate[k * zrows : (k + 1) * zrows]
-    for d in far_z:
-        to = (z + d) % nz
-        push(gate_send.at[to], gate_recv.at[z], sent.at[GZ], arrived.at[GZ], z=to)
-
-    for c in range(chunks):
-        await_all(w_flat.at[c, : (ny - 1) * 128], wy_recv.at[c])
+
+    def project(c):
         product = jnp.dot(x, w_flat[c], preferred_element_type=F32)
         for k in range(nz):
             part_send[c, k] = jnp.concatenate(
@@ -278,6 +288,44 @@
             push(
                 part_send.at[c, to], part_recv.at[c, z], sent.at[PZ], pz_recv.at[c], z=to
             )
+
+    await_all(w_flat.at[0, : (ny - 1) * 128], wy_recv.at[0])
+    project(0)
+    squares = jnp.zeros((rows, 1), F32)
+    for s in range(ny):
+        wide_rows = tok_all[s].astype(F32)
+        squares = squares + jnp.sum(wide_rows * wide_rows, axis=1, keepdims=True)
+    loads[0].wait()
+    loads[1].wait()
+    gate = jnp.concatenate(
+        [
+            lax.dot_general(x, wig[...], contract, preferred_element_type=F32),
+            lax.dot_general(x, wfg[...], contract, preferred_element_type=F32),
+            jnp.broadcast_to(squares, (rows, 96)),
+        ],
+        axis=1,
+    )
+    for k in range(nz):
+        gate_send[k] = gate[k * zrows : (k + 1) * zrows]
+    for d in far_z:
+        to = (z + d) % nz
+        push(gate_send.at[to], gate_recv.at[z], sent.at[GZ], arrived.at[GZ], z=to)
+
+    if nx > 1:
+        shared = w_flat.at[last, : (ny - 1) * (nx - 1) * some]
+        await_all(shared, arrived.at[WX])
+    project(last)
+    for c in range(1, last):
+        await_all(w_flat.at[c, : (ny - 1) * 128], wy_recv.at[c])
+        project(c)
+
+    await_all(wo_all.at[tp, share, : (ny - 1) * 128], arrived.at[OY])
+    for d in near_y:
+        there = wo_all.at[tp, share, out_columns((y + d) % ny)]
+        for e in near_x:
+            push(there, there, sent.at[OX], arrived.at[OX], dp=(x_rank + e) % nx)
+    up_copy = push(w_up, up_all.at[tp], pair_send.at[2], pair_recv.at[2], tp=other)
+    down_copy = push(w_down, down_all.at[tp], pair_send.at[3], pair_recv.at[3], tp=other)
 
     loads[2].wait()
 
@@ -341,13 +389,7 @@
     inflow = column(jnp.exp(ingate - new_stab))
     floor = column(jnp.exp(-new_stab))
 
-    for c in range(chunks):
-        if c == chunks - 1:
-            await_all(wo_all.at[tp, share, : (ny - 1) * 128], arrived.at[OY])
-            for d in near_y:
-                there = wo_all.at[tp, share, out_columns((y + d) % ny)]
-                for e in near_x:
-                    push(there, there, sent.at[OX], arrived.at[OX], dp=(x_rank + e) % nx)
+    for c in [0, last] + list(range(1, last)):
         await_all(part_recv.at[c, : nz - 1], pz_recv.at[c])
         total = part_send[c, z].astype(F32)
         for d in near_z:
@@ -379,19 +421,18 @@
     packed[2 * piece : 3 * piece] = jnp.broadcast_to(retain, (piece, 128))
     sub = lax.broadcasted_iota(jnp.int32, (heads, 128), 0)
 
-    def readout_of(b, carry):
-        here = pl.ds(pl.multiple_of(b * heads, heads), heads)
-        q_b = q_twice[here, :].astype(BF16)
-        found = jnp.zeros((heads, 128), F32)
-        for h in range(heads):
-            product = lax.dot_general(
-                q_b, mem_split[b * heads + h], contract, preferred_element_type=F32
-            )
-            found = jnp.where(sub == h, product, found)
-        mq[here, :] = found
-        return carry
-
-    lax.fori_loop(0, own, readout_of, 0)
+    for b in range(own):
+        these = slice(b * heads, (b + 1) * heads)
+        product = lax.dot_general(
+            q_twice[these, :].astype(BF16),
+            mem_split[these].reshape(heads * 128, 256),
+            contract,
+            preferred_element_type=F32,
+        )
+        found = product[:, :128]
+        for h in range(1, heads):
+            found = jnp.where(sub == h, product[:, h * 128 : (h + 1) * 128], found)
+        mq[these, :] = found
     numerator = retain * mq[...] + inflow_value * jnp.sum(key * query, axis=1, keepdims=True)
     denominator = jnp.sum(new_norm * query, axis=1, keepdims=True)
     readout = numerator / jnp.maximum(jnp.abs(denominator), floor)
@@ -427,8 +468,9 @@
 
     loads[3].wait()
     if nx > 1:
-        passed_on = wo_all.at[tp, : depth // nx * (nx - 1), : (ny - 1) * 128]
+        passed_on = wo_all.at[tp, : part * (nx - 1), : (ny - 1) * 128]
         await_all(passed_on, arrived.at[OX])
+    await_all(wo_all.at[tp, head, : (ny - 1) * 128], arrived.at[OD])
     for d in near_y:
         whole = wo_all.at[tp, :, out_columns((y + d) % ny)]
         push(whole, whole, sent.at[OP], arrived.at[OP], tp=other)
@@ -463,15 +505,20 @@
     wcols = block // 2
     mixed_all[z, y] = jnp.concatenate([mixed[:, :wcols], mixed[:, wcols:]], axis=0).astype(BF16)
 
+    mine_here = mixed_all.at[z, y]
+    for e in near_y:
+        push(mine_here, mine_here, sent.at[MY], my_recv.at[z], y=(y + e) % ny)
     for d in near_z:
-        push(
-            mixed_all.at[z, y], mixed_all.at[z, y], sent.at[MZ], mz_recv.at[z], z=(z + d) % nz
-        )
-    for d in [0] + near_z:
+        push(mine_here, mine_here, sent.at[MZ], mz_recv.at[z], z=(z + d) % nz)
+    await_all(mixed_all.at[z, : ny - 1], my_recv.at[z])
+    for e in near_y:
+        there = mixed_all.at[z, (y + e) % ny]
+        for d in next_z:
+            push(there, there, sent.at[MN], mz_recv.at[z], z=(z + d) % nz)
+    for d in rest_z:
         s = (z + d) % nz
         here = mixed_all.at[s, y]
-        if d:
-            await_all(here, mz_recv.at[s])
+        await_all(here, mz_recv.at[s])
         for e in near_y:
             push(here, here, sent.at[MY], my_recv.at[s], y=(y + e) % ny)
     loads[4].wait()
@@ -480,7 +527,10 @@
     squares = [jnp.zeros((mrows, 1), F32)] * ny
     for d in [0] + near_z:
         s = (z + d) % nz
-        await_all(mixed_all.at[s, : ny - 1], my_recv.at[s])
+        if d in next_z:
+            await_all(mixed_all.at[s], mz_recv.at[s])
+        elif d:
+            await_all(mixed_all.at[s, : ny - 1], my_recv.at[s])
         gain = jnp.concatenate([gains[1, pl.ds(s * ny + k, 1), :] for k in range(ny)], axis=1)
         scaled = []
         for k in range(ny):
@@ -503,54 +553,85 @@
 
     loads[5].wait()
     down_copy.wait_recv()
-    order = far_z + [0]
-    for d in order:
+    rest = rest_z[::-1]
+    for d in next_z + rest + [0]:
         to = (z + d) % nz
         here = pl.ds(pl.multiple_of(to * block, block), block)
         product = jnp.dot(
             squared[0], down_all[0, :, here], preferred_element_type=F32
         ) + jnp.dot(squared[1], down_all[1, :, here], preferred_element_type=F32)
         for k in range(ny):
-            down_send[to, k] = product[:, k * 128 : (k + 1) * 128].astype(BF16)
-        for e in near_y:
-            dst = (y + e) % ny
-            push(down_send.at[to, dst], down_y.at[y, to], sent.at[DY], dy_recv.at[to], y=dst)
+            piece_k = product[:, k * 128 : (k + 1) * 128]
+            if d:
+                down_send[to, k] = piece_k.astype(BF16)
+            else:
+                down_own[k] = piece_k
+        if d in next_z:
+            push(
+                down_send.at[to],
+                down_next.at[next_z.index(d)],
+                sent.at[DN],
+                arrived.at[DN],
+                z=to,
+            )
+        elif d:
+            for e in near_y:
+                dst = (y + e) % ny
+                push(
+                    down_send.at[to, dst], down_y.at[y, to], sent.at[DY], dy_recv.at[to], y=dst
+                )
+    carried = []
+    for k in range(ny):
+        stacked = mixed_all[z, k].astype(F32)
+        mine = jnp.zeros((mrows, 128), F32)
+        for c in range(ny):
+            down, across = c // (ny // 2) * mrows, c % (ny // 2) * 128
+            mine = jnp.where(y == c, stacked[down : down + mrows, across : across + 128], mine)
+        carried.append(mine)
+    carried = jnp.concatenate(carried, axis=0)
     quarter = half // 2
 
     def columns_of(value, t):
         cols = value[:, 64 * t : 64 * (t + 1)]
         return jnp.concatenate([cols[:quarter], cols[quarter:]], axis=1)
 
-    for d in order:
+    def add_next():
+        await_all(down_next, arrived.at[DN])
+        for k in range(ny):
+            added = down_own[k]
+            for i in range(len(next_z)):
+                added = added + down_next[i, k].astype(F32)
+            down_own[k] = added
+            down_send[z, k] = added.astype(BF16)
+        for e in near_y:
+            dst = (y + e) % ny
+            push(down_send.at[z, dst], down_y.at[y, z], sent.at[DY], dy_recv.at[z], y=dst)
+
+    if not rest:
+        add_next()
+    for d in rest + [0]:
         to = (z + d) % nz
         await_all(down_y.at[: ny - 1, to], dy_recv.at[to])
-        summed = down_send[to, y].astype(F32)
+        summed = down_send[to, y].astype(F32) if d else down_own[y]
         for e in near_y:
             summed = summed + down_y[(y + e) % ny, to].astype(F32)
         if d:
             for t in range(2):
                 sum_send[t, to] = columns_of(summed, t).astype(BF16)
                 push(sum_send.at[t, to], sum_recv.at[tp, z], sent.at[DZ], arrived.at[DZ], z=to, tp=t)
+            if d == rest[0]:
+                add_next()
         else:
-            carried = []
-            for k in range(ny):
-                stacked = mixed_all[z, k].astype(F32)
-                mine = jnp.zeros((mrows, 128), F32)
-                for c in range(ny):
-                    down, across = c // (ny // 2) * mrows, c % (ny // 2) * 128
-                    mine = jnp.where(
-                        y == c, stacked[down : down + mrows, across : across + 128], mine
-                    )
-                carried.append(mine)
-            whole = summed + jnp.concatenate(carried, axis=0)
+            whole = summed + carried
             fin_send[0] = columns_of(whole, 0)
             fin_send[1] = columns_of(whole, 1)
             fin_copy = push(
                 fin_send.at[other], fin_recv, pair_send.at[4], pair_recv.at[4], tp=other
             )
-    await_all(sum_recv.at[:, : nz - 1], arrived.at[DZ])
+    if rest:
+        await_all(sum_recv.at[:, : len(rest)], arrived.at[DZ])
     total = [fin_send[tp], jnp.zeros((quarter, 128), F32)]
-    for d in near_z:
+    for d in rest:
         src = (z + d) % nz
         total[0] = total[0] + sum_recv[tp, src].astype(F32)
         total[1] = total[1] + sum_recv[other, src].astype(F32)
@@ -562,19 +643,25 @@
 
     for copy in (tok_copy, out_copy, up_copy, down_copy, fin_copy):
         copy.wait_send()
-    await_sent(w_own.at[: ny - 1], sent.at[WY])
+    await_sent(w_own.at[: ny - 1, :last], sent.at[WY])
+    await_sent(w_flat.at[last, : (ny - 1) * some], sent.at[WQ])
+    await_sent(wo_all.at[tp, head, : (ny - 1) * 128], sent.at[OD])
     await_sent(tok_all.at[: ny - 1], sent.at[TY])
     await_sent(part_send.at[:, : nz - 1], sent.at[PZ])
     await_sent(gate_send.at[: nz - 1], sent.at[GZ])
     await_sent(rows_send.at[: ny - 1], sent.at[RY])
     await_sent(wo_all.at[tp, share, : (ny - 1) * 128], sent.at[OY])
     if nx > 1:
+        await_sent(shared, sent.at[WX])
         await_sent(passed_on, sent.at[OX])
     await_sent(wo_all.at[tp, :, : (ny - 1) * 128], sent.at[OP])
     await_sent(mixed_all.at[: nz - 1, 0], sent.at[MZ])
-    await_sent(mixed_all.at[:, : ny - 1], sent.at[MY])
-    await_sent(down_send.at[:, : ny - 1], sent.at[DY])
-    await_sent(sum_send.at[:, : nz - 1], sent.at[DZ])
+    await_sent(mixed_all.at[: len(next_z), : ny - 1], sent.at[MN])
+    await_sent(mixed_all.at[: nz - len(next_z), : ny - 1], sent.at[MY])
+    await_sent(down_next, sent.at[DN])
+    await_sent(down_send.at[: nz - len(next_z), : ny - 1], sent.at[DY])
+    if rest:
+        await_sent(sum_send.at[:, : len(rest)], sent.at[DZ])
 
     @pl.when(tp == core)
     def _():
@@ -585,30 +672,27 @@
         await_sent(heads_all, sent.at[HZ])
 
 
-def update(ny, mem, packed, new_mem, out, norm, stab, made, sems):
-    count = sems.shape[0]
+def update(ny, mem, packed_hbm, new_mem, out_hbm, norm_hbm, stab_hbm, packed, made, out, stab, sems):
+    load = pltpu.make_async_copy(packed_hbm, packed, sems.at[0])
+    load.start()
     piece = mem.shape[0]
+    own = stab.shape[0]
+    count = sems.shape[0] - 4
     each = piece // count
-    inflow_v = packed[:piece].T
     copies = []
-    for b in range(count):
-        for i in range(b * each, (b + 1) * each):
-            key, retain = packed[piece + i], packed[2 * piece + i]
-            made[i] = retain[None] * mem[i] + inflow_v[:, i : i + 1] * key[None]
-        here = pl.ds(b * each, each)
-        copies.append(pltpu.make_async_copy(made.at[here], new_mem.at[here], sems.at[b]))
+
+    def send(src, dst):
+        copies.append(pltpu.make_async_copy(src, dst, sems.at[1 + len(copies)]))
         copies[-1].start()
-    norm[...] = packed[3 * piece : 4 * piece]
-    stab[...] = packed[4 * piece : 4 * piece + stab.shape[0], : stab.shape[1]]
+
     rows = out.shape[1]
-    own, blocks = stab.shape[0], rows // stab.shape[0] // 2
+    blocks = rows // own // 2
     per = blocks // ny
     quarter = rows // 4
     line = lax.broadcasted_iota(jnp.int32, (rows // 2, rows), 0).astype(F32)
     column = lax.broadcasted_iota(jnp.int32, (rows // 2, rows), 1).astype(F32)
     side = jnp.where(line >= quarter, 1.0, 0.0)
-    result = packed[4 * piece + 8 :].T.astype(BF16)
-    turned = jnp.zeros((64, rows), F32)
+    orders = []
     for upper in range(2):
         at = line + side * quarter + upper * quarter
         group = jnp.floor((at + 0.5) / own)
@@ -616,11 +700,25 @@
         in_y = jnp.floor((inner + 0.5) / per)
         in_z = inner - in_y * per
         target = (side * blocks + in_z * ny + in_y) * own + (at - group * own)
-        order = jnp.where(column == target, 1.0, 0.0).astype(BF16)
-        turned = turned + jnp.dot(
-            result[64 * upper : 64 * (upper + 1)], order, preferred_element_type=F32
-        )
-    out[...] = turned.astype(BF16)
+        orders.append(jnp.where(column == target, 1.0, 0.0).astype(BF16))
+    load.wait()
+    inflow_v = packed[:piece].T
+    for b in range(count):
+        for i in range(b * each, (b + 1) * each):
+            key, retain = packed[piece + i], packed[2 * piece + i]
+            made[i] = retain[None] * mem[i] + inflow_v[:, i : i + 1] * key[None]
+        here = pl.ds(b * each, each)
+        send(made.at[here], new_mem.at[here])
+        if b == 0:
+            send(packed.at[pl.ds(3 * piece, piece)], norm_hbm)
+            stab[...] = packed[4 * piece : 4 * piece + own, : stab.shape[1]]
+            send(stab, stab_hbm)
+            result = packed[4 * piece + 8 :].T.astype(BF16)
+            turned = jnp.dot(result[:64], orders[0], preferred_element_type=F32) + jnp.dot(
+                result[64:], orders[1], preferred_element_type=F32
+            )
+            out[...] = turned.astype(BF16)
+            send(out, out_hbm)
     for copy in copies:
         copy.wait()
 
@@ -707,6 +805,8 @@
             pltpu.VMEM((nz, ny, 2 * mrows, block // 2), BF16),
             pltpu.VMEM((2, half, weight_up.shape[1]), F32),
             pltpu.VMEM((nz, ny, half, 128), BF16),
+            pltpu.VMEM((ny, half, 128), F32),
+            pltpu.VMEM((min(2, nz - 1), ny, half, 128), BF16),
             pltpu.VMEM((ny, nz, half, 128), BF16),
             pltpu.VMEM((2, nz, half // 2, 128), BF16),
             pltpu.VMEM((2, nz, half // 2, 128), BF16),
@@ -748,9 +848,15 @@
             jax.ShapeDtypeStruct((piece, hd), F32),
             jax.ShapeDtypeStruct((own, heads), F32),
         ),
-        in_specs=[vmem] * 2,
-        out_specs=(hbm, vmem, vmem, vmem),
-        scratch_shapes=[pltpu.VMEM(mem48.shape, F32), dma((own,))],
+        in_specs=[vmem, pl.BlockSpec(memory_space=pltpu.HBM)],
+        out_specs=(hbm,) * 4,
+        scratch_shapes=[
+            pltpu.VMEM(packed.shape, F32),
+            pltpu.VMEM(mem48.shape, F32),
+            pltpu.VMEM(tokens.shape, BF16),
+            pltpu.VMEM((own, heads), F32),
+            dma((piece // 4 + 4,)),
+        ],
         compiler_params=pltpu.CompilerParams(vmem_limit_bytes=16 * 1024 * 1024),
     )(mem48, packed)
     new_memory = new_memory.reshape(memory.shape)

time: 74.8 us -> 72 us (0.963)
  Pallas kernels: 73.1 us -> 70.3 us
    pallas_call x1, Pallas kernels: 70.4 us -> 68 us  [body(): pl.pallas_call(functools.partial(kernel, nx, nz, ny, width_full), out_sha...]
where the time goes in v4:
time: 72 us; the launch traced here: 71.9 us
  Pallas kernels  70.3 us (98%)
  local copies, waits for them, and re-layouts  0.91 us (1%)
    pallas_call x1, Pallas kernels, body(): pl.pallas_call(functools.partial(kernel, nx, nz, ny, width_full), out_sha...  68 us
    pallas_call x1, Pallas kernels, body(): pl.pallas_call(functools.partial(update, ny), out_shape=(jax.ShapeDtypeSt...  2.29 us

profile of v4, /device:TPU:1, one launch (start us, length us, event | category | flops | bytes accessed | tf_op | source)
XLA Modules:
  0.0 71.9 jit_solution(11704615137539314322)
XLA Ops:
  0.6 0.0 copy-start
  0.6 68.0 %shard_map.201.packed_hbm = f32[296,128]{1,0:T(8,128)} custom-call(bf16[64,192]{1,0:T(8,128)(2,1)} %bitcast.16, bf16[32,128]{1,0:T(8,128)(2,1)} %bitcast.18, f32[1,16]{1,0:T(1,128)} %bitcast.20, f32[1,16]{1,0:T(1,128)} %bitcast.21, f32[48,128]{1,0:T(8,128)} %bitcast.17, f32[6,8]{1,0:T(8,128)} %stabilizer_hbm.1, bf16[16,128]{1,0:T(8,128)(2,1)} %head_gain_hbm.1, ...), custom_call_target="tpu_custom_call" | custom-call | tf_op jit(solution)/shard_map/pallas_call | solution.py:771
  68.7 0.0 copy-done
  68.7 0.0 copy-start.1
  68.7 0.9 %copy-done.1 = f32[296,128]{1,0:T(8,128)S(1)} copy-done((f32[296,128]{1,0:T(8,128)S(1)}, f32[296,128]{1,0:T(8,128)}, u32[]{:S(2)}) %copy-start.1) | copy-done | bytes 151576
  69.6 2.3 %shard_map.202 = (f32[48,128,128]{2,1,0:T(8,128)}, bf16[64,192]{1,0:T(8,128)(2,1)}, f32[48,128]{1,0:T(8,128)}, f32[6,8]{1,0:T(8,128)}) custom-call(f32[48,128,128]{2,1,0:T(8,128)S(1)} %bitcast.13, f32[296,128]{1,0:T(8,128)S(1)} %copy-done.1), custom_call_target="tpu_custom_call" | custom-call | tf_op jit(solution)/shard_map/pallas_call | solution.py:843
Async XLA Ops:
  0.6 68.0 %copy-start = (f32[6,8,128,128]{3,2,1,0:T(8,128)S(1)}, f32[6,8,128,128]{3,2,1,0:T(8,128)}, u32[]{:S(2)}) copy-start(f32[6,8,128,128]{3,2,1,0:T(8,128)} %param.28) | copy-start | bytes 9437188
  68.7 0.9 %copy-start.1 = (f32[296,128]{1,0:T(8,128)S(1)}, f32[296,128]{1,0:T(8,128)}, u32[]{:S(2)}) copy-start(f32[296,128]{1,0:T(8,128)} %shard_map.201.packed_hbm) | copy-start | bytes 454660

commit v5 on v4

--- a/solution.py
+++ b/solution.py
@@ -215,18 +215,17 @@
                 y=to,
             )
 
-    last = chunks - 1
+    direct_chunks = chunks // 2
     some = 128 // nx
 
     def share_of(k):
         return pl.ds(pl.multiple_of(k * 128 + x_rank * some, some), some)
 
-    send_chunk(0)
     for d in near_y:
         to = (y + d) % ny
         push(
-            w_own.at[to, last, share_of(0)],
-            w_flat.at[last, share_of(y)],
+            w_own.at[to, direct_chunks:, share_of(0)],
+            w_flat.at[direct_chunks:, share_of(y)],
             sent.at[WQ],
             arrived.at[WQ],
             y=to,
@@ -243,7 +242,7 @@
         push(
             tok_all.at[y], tok_all.at[y], sent.at[TY], arrived.at[TY], y=(y + d) % ny
         )
-    for c in range(1, last):
+    for c in range(direct_chunks):
         send_chunk(c)
     direct = depth // 2
     part = (depth - direct) // nx
@@ -259,11 +258,13 @@
     out_copy = push(w_out, own_out, pair_send.at[1], pair_recv.at[1], tp=other)
     for c in range(chunks):
         w_flat[c, own_block] = w_own[y, c]
-    await_all(w_flat.at[last, : (ny - 1) * some], arrived.at[WQ])
-    for d in near_y:
-        there = w_flat.at[last, share_of((y + d) % ny)]
-        for e in near_x:
-            push(there, there, sent.at[WX], arrived.at[WX], dp=(x_rank + e) % nx)
+    await_all(w_flat.at[direct_chunks:, : (ny - 1) * some], arrived.at[WQ])
+    shared_chunks = range(direct_chunks, chunks)
+    for c in shared_chunks:
+        for d in near_y:
+            there = w_flat.at[c, share_of((y + d) % ny)]
+            for e in near_x:
+                push(there, there, sent.at[WX], wy_recv.at[c], dp=(x_rank + e) % nx)
     await_all(tok_all.at[: ny - 1], arrived.at[TY])
     x = jnp.concatenate(
         [
@@ -289,8 +290,6 @@
                 part_send.at[c, to], part_recv.at[c, z], sent.at[PZ], pz_recv.at[c], z=to
             )
 
-    await_all(w_flat.at[0, : (ny - 1) * 128], wy_recv.at[0])
-    project(0)
     squares = jnp.zeros((rows, 1), F32)
     for s in range(ny):
         wide_rows = tok_all[s].astype(F32)
@@ -301,22 +300,23 @@
         [
             lax.dot_general(x, wig[...], contract, preferred_element_type=F32),
             lax.dot_general(x, wfg[...], contract, preferred_element_type=F32),
-            jnp.broadcast_to(squares, (rows, 96)),
+            jnp.broadcast_to(squares, (rows, 8)),
         ],
         axis=1,
     )
     for k in range(nz):
-        gate_send[k] = gate[k * zrows : (k + 1) * zrows]
+        groups = [gate[k * zrows + g * 8 : k * zrows + (g + 1) * 8] for g in range(zrows // 8)]
+        gate_send[k] = jnp.concatenate(groups + [jnp.zeros((8, 128 - 5 * zrows), F32)], axis=1)
     for d in far_z:
         to = (z + d) % nz
         push(gate_send.at[to], gate_recv.at[z], sent.at[GZ], arrived.at[GZ], z=to)
 
-    if nx > 1:
-        shared = w_flat.at[last, : (ny - 1) * (nx - 1) * some]
-        await_all(shared, arrived.at[WX])
-    project(last)
-    for c in range(1, last):
-        await_all(w_flat.at[c, : (ny - 1) * 128], wy_recv.at[c])
+    sequence = [direct_chunks, 0] + list(range(direct_chunks + 1, chunks)) + list(range(1, direct_chunks))
+    for c in sequence:
+        if c < direct_chunks:
+            await_all(w_flat.at[c, : (ny - 1) * 128], wy_recv.at[c])
+        elif nx > 1:
+            await_all(w_flat.at[c, : (ny - 1) * (nx - 1) * some], wy_recv.at[c])
         project(c)
 
     await_all(wo_all.at[tp, share, : (ny - 1) * 128], arrived.at[OY])
@@ -355,9 +355,12 @@
     gate_sum = gate_send[z]
     for d in near_z:
         gate_sum = gate_sum + gate_recv[(z + d) % nz]
+    gate_sum = jnp.concatenate(
+        [gate_sum[:, g * 40 : (g + 1) * 40] for g in range(zrows // 8)], axis=0
+    )
     inverse = lax.rsqrt(gate_sum[:, 32:33] / width_full + EPS)
     gate_pre = inverse * gate_sum
-    gate_rows = jnp.zeros((own, 128), F32)
+    gate_rows = jnp.zeros((own, 40), F32)
     for k in range(ny):
         gate_rows = gate_rows + jnp.where(y == k, gate_pre[k * own : (k + 1) * own], 0.0)
     in_all = gate_rows[:, 0:16] + bias_in[...]
@@ -389,7 +392,7 @@
     inflow = column(jnp.exp(ingate - new_stab))
     floor = column(jnp.exp(-new_stab))
 
-    for c in [0, last] + list(range(1, last)):
+    for c in sequence:
         await_all(part_recv.at[c, : nz - 1], pz_recv.at[c])
         total = part_send[c, z].astype(F32)
         for d in near_z:
@@ -508,7 +511,7 @@
     mine_here = mixed_all.at[z, y]
     for e in near_y:
         push(mine_here, mine_here, sent.at[MY], my_recv.at[z], y=(y + e) % ny)
-    for d in near_z:
+    for d in rest_z + next_z:
         push(mine_here, mine_here, sent.at[MZ], mz_recv.at[z], z=(z + d) % nz)
     await_all(mixed_all.at[z, : ny - 1], my_recv.at[z])
     for e in near_y:
@@ -554,7 +557,7 @@
     loads[5].wait()
     down_copy.wait_recv()
     rest = rest_z[::-1]
-    for d in next_z + rest + [0]:
+    for d in rest[:1] + next_z + rest[1:] + [0]:
         to = (z + d) % nz
         here = pl.ds(pl.multiple_of(to * block, block), block)
         product = jnp.dot(
@@ -643,8 +646,8 @@
 
     for copy in (tok_copy, out_copy, up_copy, down_copy, fin_copy):
         copy.wait_send()
-    await_sent(w_own.at[: ny - 1, :last], sent.at[WY])
-    await_sent(w_flat.at[last, : (ny - 1) * some], sent.at[WQ])
+    await_sent(w_own.at[: ny - 1, :direct_chunks], sent.at[WY])
+    await_sent(w_flat.at[direct_chunks:, : (ny - 1) * some], sent.at[WQ])
     await_sent(wo_all.at[tp, head, : (ny - 1) * 128], sent.at[OD])
     await_sent(tok_all.at[: ny - 1], sent.at[TY])
     await_sent(part_send.at[:, : nz - 1], sent.at[PZ])
@@ -652,7 +655,7 @@
     await_sent(rows_send.at[: ny - 1], sent.at[RY])
     await_sent(wo_all.at[tp, share, : (ny - 1) * 128], sent.at[OY])
     if nx > 1:
-        await_sent(shared, sent.at[WX])
+        await_sent(w_flat.at[direct_chunks:, : (ny - 1) * (nx - 1) * some], sent.at[WX])
         await_sent(passed_on, sent.at[OX])
     await_sent(wo_all.at[tp, :, : (ny - 1) * 128], sent.at[OP])
     await_sent(mixed_all.at[: nz - 1, 0], sent.at[MZ])
@@ -789,8 +792,8 @@
             pltpu.VMEM((chunks, block, 2 * hd), BF16),
             pltpu.VMEM((chunks, nz, 2 * zrows, hd), BF16),
             pltpu.VMEM((chunks, nz, 2 * zrows, hd), BF16),
-            pltpu.VMEM((nz, zrows, 128), F32),
-            pltpu.VMEM((nz, zrows, 128), F32),
+            pltpu.VMEM((nz, 8, 128), F32),
+            pltpu.VMEM((nz, 8, 128), F32),
             pltpu.VMEM((zrows * heads, hd), F32),
             pltpu.VMEM((ny, piece, hd), BF16),
             pltpu.VMEM((ny, piece, hd), BF16),

time: 72 us -> 70 us (0.972)
  Pallas kernels: 70.3 us -> 68.3 us
    pallas_call x1, Pallas kernels: 68 us -> 66.1 us  [body(): pl.pallas_call(functools.partial(kernel, nx, nz, ny, width_full), out_sha...]
where the time goes in v5:
time: 70 us; the launch traced here: 69.9 us
  Pallas kernels  68.3 us (98%)
  local copies, waits for them, and re-layouts  0.91 us (1%)
    pallas_call x1, Pallas kernels, body(): pl.pallas_call(functools.partial(kernel, nx, nz, ny, width_full), out_sha...  66.1 us
    pallas_call x1, Pallas kernels, body(): pl.pallas_call(functools.partial(update, ny), out_shape=(jax.ShapeDtypeSt...  2.29 us

profile of v5, /device:TPU:1, one launch (start us, length us, event | category | flops | bytes accessed | tf_op | source)
XLA Modules:
  0.0 69.9 jit_solution(7161540966488083818)
XLA Ops:
  0.6 0.0 copy-start
  0.6 66.1 %shard_map.201.packed_hbm = f32[296,128]{1,0:T(8,128)} custom-call(bf16[64,192]{1,0:T(8,128)(2,1)} %bitcast.16, bf16[32,128]{1,0:T(8,128)(2,1)} %bitcast.18, f32[1,16]{1,0:T(1,128)} %bitcast.20, f32[1,16]{1,0:T(1,128)} %bitcast.21, f32[48,128]{1,0:T(8,128)} %bitcast.17, f32[6,8]{1,0:T(8,128)} %stabilizer_hbm.1, bf16[16,128]{1,0:T(8,128)(2,1)} %head_gain_hbm.1, ...), custom_call_target="tpu_custom_call" | custom-call | tf_op jit(solution)/shard_map/pallas_call | solution.py:774
  66.7 0.0 copy-done
  66.7 0.0 copy-start.1
  66.7 0.9 %copy-done.1 = f32[296,128]{1,0:T(8,128)S(1)} copy-done((f32[296,128]{1,0:T(8,128)S(1)}, f32[296,128]{1,0:T(8,128)}, u32[]{:S(2)}) %copy-start.1) | copy-done | bytes 151576
  67.6 2.3 %shard_map.202 = (f32[48,128,128]{2,1,0:T(8,128)}, bf16[64,192]{1,0:T(8,128)(2,1)}, f32[48,128]{1,0:T(8,128)}, f32[6,8]{1,0:T(8,128)}) custom-call(f32[48,128,128]{2,1,0:T(8,128)S(1)} %bitcast.13, f32[296,128]{1,0:T(8,128)S(1)} %copy-done.1), custom_call_target="tpu_custom_call" | custom-call | tf_op jit(solution)/shard_map/pallas_call | solution.py:846
Async XLA Ops:
  0.6 66.1 %copy-start = (f32[6,8,128,128]{3,2,1,0:T(8,128)S(1)}, f32[6,8,128,128]{3,2,1,0:T(8,128)}, u32[]{:S(2)}) copy-start(f32[6,8,128,128]{3,2,1,0:T(8,128)} %param.28) | copy-start | bytes 9437188
  66.7 0.9 %copy-start.1 = (f32[296,128]{1,0:T(8,128)S(1)}, f32[296,128]{1,0:T(8,128)}, u32[]{:S(2)}) copy-start(f32[296,128]{1,0:T(8,128)} %shard_map.201.packed_hbm) | copy-start | bytes 454660

commit v6 on v5

--- a/solution.py
+++ b/solution.py
@@ -98,6 +98,7 @@
     sent,
     arrived,
     wy_recv,
+    wq_recv,
     pz_recv,
     mz_recv,
     my_recv,
@@ -187,18 +188,21 @@
     for copy in raw_loads + small:
         copy.start()
     chunks = heads // 2
+    direct_chunks = chunks // 2
+    shared_chunks = range(direct_chunks, chunks)
+
+    def flatten(m, which):
+        for c in which:
+            for i in range(2):
+                w_own[m, c, :, i * 128 : (i + 1) * 128] = wide[
+                    m, pl.ds(2 * c + i, 128, stride=heads), :
+                ].astype(BF16)
+
     for m in range(4):
         raw_loads[m].wait()
-        wide[...] = w_raw[m].astype(F32).reshape(128 * heads, 128)
-        for h in range(heads):
-            w_own[m, h // 2, :, (h % 2) * 128 : (h % 2 + 1) * 128] = wide[
-                pl.ds(h, 128, stride=heads), :
-            ].astype(BF16)
-    for copy in small:
-        copy.wait()
-    gains[0] = gain_mixer[...].astype(F32)
-    gains[1] = gain_channel[...].astype(F32)
-
+        wide[m] = w_raw[m].astype(F32).reshape(128 * heads, 128)
+        flatten(m, shared_chunks)
+    small[0].wait()
     pl.semaphore_wait(barrier, 2 * (nz - 1) + (ny - 1) + (nx - 1) + 1)
 
     tok_copy = push(tokens, tok_in, pair_send.at[0], pair_recv.at[0], tp=other)
@@ -215,23 +219,25 @@
                 y=to,
             )
 
-    direct_chunks = chunks // 2
     some = 128 // nx
 
     def share_of(k):
         return pl.ds(pl.multiple_of(k * 128 + x_rank * some, some), some)
 
-    for d in near_y:
-        to = (y + d) % ny
-        push(
-            w_own.at[to, direct_chunks:, share_of(0)],
-            w_flat.at[direct_chunks:, share_of(y)],
-            sent.at[WQ],
-            arrived.at[WQ],
-            y=to,
-        )
+    for c in shared_chunks:
+        for d in near_y:
+            to = (y + d) % ny
+            push(
+                w_own.at[to, c, share_of(0)], w_flat.at[c, share_of(y)], sent.at[WQ], wq_recv.at[c], y=to
+            )
     for copy in loads:
         copy.start()
+    for m in range(4):
+        flatten(m, range(direct_chunks))
+    for copy in small[1:]:
+        copy.wait()
+    gains[0] = gain_mixer[...].astype(F32)
+    gains[1] = gain_channel[...].astype(F32)
     tok_copy.wait_recv()
     mine, theirs = tokens[...].astype(F32), tok_in[...].astype(F32)
     first = jnp.where(tp == 0, mine, theirs)
@@ -258,9 +264,8 @@
     out_copy = push(w_out, own_out, pair_send.at[1], pair_recv.at[1], tp=other)
     for c in range(chunks):
         w_flat[c, own_block] = w_own[y, c]
-    await_all(w_flat.at[direct_chunks:, : (ny - 1) * some], arrived.at[WQ])
-    shared_chunks = range(direct_chunks, chunks)
     for c in shared_chunks:
+        await_all(w_flat.at[c, : (ny - 1) * some], wq_recv.at[c])
         for d in near_y:
             there = w_flat.at[c, share_of((y + d) % ny)]
             for e in near_x:
@@ -675,36 +680,17 @@
         await_sent(heads_all, sent.at[HZ])
 
 
-def update(ny, mem, packed_hbm, new_mem, out_hbm, norm_hbm, stab_hbm, packed, made, out, stab, sems):
-    load = pltpu.make_async_copy(packed_hbm, packed, sems.at[0])
-    load.start()
+def update(ny, mem, packed, new_mem, out_hbm, norm_hbm, stab_hbm, made, out, stab, sems):
     piece = mem.shape[0]
     own = stab.shape[0]
-    count = sems.shape[0] - 4
+    count = sems.shape[0] - 3
     each = piece // count
     copies = []
 
     def send(src, dst):
-        copies.append(pltpu.make_async_copy(src, dst, sems.at[1 + len(copies)]))
+        copies.append(pltpu.make_async_copy(src, dst, sems.at[len(copies)]))
         copies[-1].start()
 
-    rows = out.shape[1]
-    blocks = rows // own // 2
-    per = blocks // ny
-    quarter = rows // 4
-    line = lax.broadcasted_iota(jnp.int32, (rows // 2, rows), 0).astype(F32)
-    column = lax.broadcasted_iota(jnp.int32, (rows // 2, rows), 1).astype(F32)
-    side = jnp.where(line >= quarter, 1.0, 0.0)
-    orders = []
-    for upper in range(2):
-        at = line + side * quarter + upper * quarter
-        group = jnp.floor((at + 0.5) / own)
-        inner = group - side * blocks
-        in_y = jnp.floor((inner + 0.5) / per)
-        in_z = inner - in_y * per
-        target = (side * blocks + in_z * ny + in_y) * own + (at - group * own)
-        orders.append(jnp.where(column == target, 1.0, 0.0).astype(BF16))
-    load.wait()
     inflow_v = packed[:piece].T
     for b in range(count):
         for i in range(b * each, (b + 1) * each):
@@ -716,6 +702,22 @@
             send(packed.at[pl.ds(3 * piece, piece)], norm_hbm)
             stab[...] = packed[4 * piece : 4 * piece + own, : stab.shape[1]]
             send(stab, stab_hbm)
+            rows = out.shape[1]
+            blocks = rows // own // 2
+            per = blocks // ny
+            quarter = rows // 4
+            line = lax.broadcasted_iota(jnp.int32, (rows // 2, rows), 0).astype(F32)
+            column = lax.broadcasted_iota(jnp.int32, (rows // 2, rows), 1).astype(F32)
+            side = jnp.where(line >= quarter, 1.0, 0.0)
+            orders = []
+            for upper in range(2):
+                at = line + side * quarter + upper * quarter
+                group = jnp.floor((at + 0.5) / own)
+                inner = group - side * blocks
+                in_y = jnp.floor((inner + 0.5) / per)
+                in_z = inner - in_y * per
+                target = (side * blocks + in_z * ny + in_y) * own + (at - group * own)
+                orders.append(jnp.where(column == target, 1.0, 0.0).astype(BF16))
             result = packed[4 * piece + 8 :].T.astype(BF16)
             turned = jnp.dot(result[:64], orders[0], preferred_element_type=F32) + jnp.dot(
                 result[64:], orders[1], preferred_element_type=F32
@@ -787,7 +789,7 @@
             pltpu.VMEM((piece, hd, hd), F32),
             pltpu.VMEM((piece, hd, 2 * hd), BF16),
             pltpu.VMEM((ny, 128, heads, hd), BF16),
-            pltpu.VMEM((128 * heads, hd), F32),
+            pltpu.VMEM((4, 128 * heads, hd), F32),
             pltpu.VMEM((ny, chunks, 128, 2 * hd), BF16),
             pltpu.VMEM((chunks, block, 2 * hd), BF16),
             pltpu.VMEM((chunks, nz, 2 * zrows, hd), BF16),
@@ -823,6 +825,7 @@
             dma((len(PHASES),)),
             dma((chunks,)),
             dma((chunks,)),
+            dma((chunks,)),
             dma((nz,)),
             dma((nz,)),
             dma((nz,)),
@@ -851,14 +854,13 @@
             jax.ShapeDtypeStruct((piece, hd), F32),
             jax.ShapeDtypeStruct((own, heads), F32),
         ),
-        in_specs=[vmem, pl.BlockSpec(memory_space=pltpu.HBM)],
+        in_specs=[vmem, vmem],
         out_specs=(hbm,) * 4,
         scratch_shapes=[
-            pltpu.VMEM(packed.shape, F32),
             pltpu.VMEM(mem48.shape, F32),
             pltpu.VMEM(tokens.shape, BF16),
             pltpu.VMEM((own, heads), F32),
-            dma((piece // 4 + 4,)),
+            dma((piece // 4 + 3,)),
         ],
         compiler_params=pltpu.CompilerParams(vmem_limit_bytes=16 * 1024 * 1024),
     )(mem48, packed)

time: 70 us -> 68.6 us (0.980)
  Pallas kernels: 68.3 us -> 66.9 us
    pallas_call x1, Pallas kernels: 66.1 us -> 64.8 us  [body(): pl.pallas_call(functools.partial(kernel, nx, nz, ny, width_full), out_sha...]
where the time goes in v6:
time: 68.6 us; the launch traced here: 68.5 us
  Pallas kernels  66.9 us (98%)
  local copies, waits for them, and re-layouts  0.91 us (1%)
    pallas_call x1, Pallas kernels, body(): pl.pallas_call(functools.partial(kernel, nx, nz, ny, width_full), out_sha...  64.8 us
    pallas_call x1, Pallas kernels, body(): pl.pallas_call(functools.partial(update, ny), out_shape=(jax.ShapeDtypeSt...  2.07 us

profile of v6, /device:TPU:1, one launch (start us, length us, event | category | flops | bytes accessed | tf_op | source)
XLA Modules:
  0.0 68.5 jit_solution(6577330120633241666)
XLA Ops:
  0.6 0.0 copy-start
  0.6 64.8 %shard_map.201.packed = f32[296,128]{1,0:T(8,128)} custom-call(bf16[64,192]{1,0:T(8,128)(2,1)} %bitcast.16, bf16[32,128]{1,0:T(8,128)(2,1)} %bitcast.18, f32[1,16]{1,0:T(1,128)} %bitcast.20, f32[1,16]{1,0:T(1,128)} %bitcast.21, f32[48,128]{1,0:T(8,128)} %bitcast.17, f32[6,8]{1,0:T(8,128)} %stabilizer_hbm.1, bf16[16,128]{1,0:T(8,128)(2,1)} %head_gain_hbm.1, ...), custom_call_target="tpu_custom_call" | custom-call | tf_op jit(solution)/shard_map/pallas_call | solution.py:776
  65.5 0.0 copy-done
  65.5 0.0 copy-start.1
  65.5 0.9 %copy-done.1 = f32[296,128]{1,0:T(8,128)S(1)} copy-done((f32[296,128]{1,0:T(8,128)S(1)}, f32[296,128]{1,0:T(8,128)}, u32[]{:S(2)}) %copy-start.1) | copy-done | bytes 151576
  66.4 2.1 %shard_map.202 = (f32[48,128,128]{2,1,0:T(8,128)}, bf16[64,192]{1,0:T(8,128)(2,1)}, f32[48,128]{1,0:T(8,128)}, f32[6,8]{1,0:T(8,128)}) custom-call(f32[48,128,128]{2,1,0:T(8,128)S(1)} %bitcast.13, f32[296,128]{1,0:T(8,128)S(1)} %copy-done.1), custom_call_target="tpu_custom_call" | custom-call | tf_op jit(solution)/shard_map/pallas_call | solution.py:849
Async XLA Ops:
  0.6 64.8 %copy-start = (f32[6,8,128,128]{3,2,1,0:T(8,128)S(1)}, f32[6,8,128,128]{3,2,1,0:T(8,128)}, u32[]{:S(2)}) copy-start(f32[6,8,128,128]{3,2,1,0:T(8,128)} %param.28) | copy-start | bytes 9437188
  65.5 0.9 %copy-start.1 = (f32[296,128]{1,0:T(8,128)S(1)}, f32[296,128]{1,0:T(8,128)}, u32[]{:S(2)}) copy-start(f32[296,128]{1,0:T(8,128)} %shard_map.201.packed) | copy-start | bytes 454660

commit v7 on v6

--- a/solution.py
+++ b/solution.py
@@ -117,8 +117,8 @@
     zrows = ny * own
     block = ny * 128
     near_z = by_distance(nz)
-    near_y = by_distance(ny)
-    near_x = by_distance(nx)
+    near_y = by_distance(ny)[::-1]
+    near_x = by_distance(nx)[::-1]
     far_z = near_z[::-1]
     next_z = [d for d in near_z if min(d, nz - d) == 1]
     rest_z = [d for d in near_z if d not in next_z]

time: 68.6 us -> 68.4 us (level)
  no operation moved by 1% of the time
where the time goes in v7:
time: 68.4 us; the launch traced here: 68.3 us
  Pallas kernels  66.7 us (98%)
  local copies, waits for them, and re-layouts  0.91 us (1%)
    pallas_call x1, Pallas kernels, body(): pl.pallas_call(functools.partial(kernel, nx, nz, ny, width_full), out_sha...  64.6 us
    pallas_call x1, Pallas kernels, body(): pl.pallas_call(functools.partial(update, ny), out_shape=(jax.ShapeDtypeSt...  2.07 us

profile of v7, /device:TPU:1, one launch (start us, length us, event | category | flops | bytes accessed | tf_op | source)
XLA Modules:
  0.0 68.3 jit_solution(15391287467881290399)
XLA Ops:
  0.6 0.0 copy-start
  0.6 64.6 %shard_map.201.packed = f32[296,128]{1,0:T(8,128)} custom-call(bf16[64,192]{1,0:T(8,128)(2,1)} %bitcast.16, bf16[32,128]{1,0:T(8,128)(2,1)} %bitcast.18, f32[1,16]{1,0:T(1,128)} %bitcast.20, f32[1,16]{1,0:T(1,128)} %bitcast.21, f32[48,128]{1,0:T(8,128)} %bitcast.17, f32[6,8]{1,0:T(8,128)} %stabilizer_hbm.1, bf16[16,128]{1,0:T(8,128)(2,1)} %head_gain_hbm.1, ...), custom_call_target="tpu_custom_call" | custom-call | tf_op jit(solution)/shard_map/pallas_call | solution.py:776
  65.3 0.0 copy-done
  65.3 0.0 copy-start.1
  65.3 0.9 %copy-done.1 = f32[296,128]{1,0:T(8,128)S(1)} copy-done((f32[296,128]{1,0:T(8,128)S(1)}, f32[296,128]{1,0:T(8,128)}, u32[]{:S(2)}) %copy-start.1) | copy-done | bytes 151576
  66.2 2.1 %shard_map.202 = (f32[48,128,128]{2,1,0:T(8,128)}, bf16[64,192]{1,0:T(8,128)(2,1)}, f32[48,128]{1,0:T(8,128)}, f32[6,8]{1,0:T(8,128)}) custom-call(f32[48,128,128]{2,1,0:T(8,128)S(1)} %bitcast.13, f32[296,128]{1,0:T(8,128)S(1)} %copy-done.1), custom_call_target="tpu_custom_call" | custom-call | tf_op jit(solution)/shard_map/pallas_call | solution.py:849
Async XLA Ops:
  0.6 64.6 %copy-start = (f32[6,8,128,128]{3,2,1,0:T(8,128)S(1)}, f32[6,8,128,128]{3,2,1,0:T(8,128)}, u32[]{:S(2)}) copy-start(f32[6,8,128,128]{3,2,1,0:T(8,128)} %param.28) | copy-start | bytes 9437188
  65.3 0.9 %copy-start.1 = (f32[296,128]{1,0:T(8,128)S(1)}, f32[296,128]{1,0:T(8,128)}, u32[]{:S(2)}) copy-start(f32[296,128]{1,0:T(8,128)} %shard_map.201.packed) | copy-start | bytes 454660
